TPU v7x, 512 devices: a 4x2x32 block of a 4x8x32 slice. The times are simulated.
512 devices in a mesh: grp: 2 (over y), fs: 64 (over z, core), tp: 4 (over x).
Axes of the slice: x: 4, y: 2, z: 32, core: 2. Of those that a mesh axis runs over, the one named last changes fastest.
The devices are a block of a 4x8x32 slice.
Arguments:
- tokens: bfloat16 [16384, 2048], P(('grp', 'fs'), 'tp'), parts along dimension 0, may hold values from -300 to 300
- routes: int32 [16384, 8], P(('grp', 'fs')), parts along dimension 0, may hold values from 0 to 63, all different within a row; in each aligned block of 128 rows (0 to 127, 128 to 255, ...) at most 32 rows name the same one
- route_scores: float32 [16384, 8], P(('grp', 'fs')), parts along dimension 0, may hold values from 0.05 to 1
- norm_gain: float32 [2048], P('fs'), may hold values from 0.1 to 1.9
- expert_gate: float32 [64, 2048, 256], P(None, 'fs', 'tp'), may hold values from -6 to 6
- expert_up: float32 [64, 2048, 256], P(None, 'fs', 'tp'), may hold values from -6 to 6
- expert_down: float32 [64, 2048, 256], P(None, 'fs', 'tp'), may hold values from -6 to 6
- shared_gate: float32 [2048, 256], P('fs', 'tp'), may hold values from -6 to 6
- shared_up: float32 [2048, 256], P('fs', 'tp'), may hold values from -6 to 6
- shared_down: float32 [2048, 256], P('fs', 'tp'), may hold values from -6 to 6
Outputs:
- served_gate: bfloat16 [128, 2048, 256], P(('grp', 'fs'), 'tp'), parts along dimension 0
- served_up: bfloat16 [128, 2048, 256], P(('grp', 'fs'), 'tp'), parts along dimension 0
- served_down: bfloat16 [128, 2048, 256], P(('grp', 'fs'), 'tp'), parts along dimension 0
- common_gate: bfloat16 [4096, 256], P(('grp', 'tp')), parts along dimension 0
- common_up: bfloat16 [4096, 256], P(('grp', 'tp')), parts along dimension 0
- common_down: bfloat16 [4096, 256], P(('grp', 'tp')), parts along dimension 0
- mixture: bfloat16 [16384, 2048], P(('grp', 'fs'), 'tp'), parts along dimension 0
There are 2 independent parts, one for each index of `grp`. A program takes and returns all parts, laid end to end along the dimension named above; an argument that names none is the same for every part. Nothing has to cross between parts.
Inputs may be any that keep to these rules, and one draw needn't show every extreme that they name: `routes`: each row names 8 different experts. Within the rows of one index of fs (aligned blocks of 128 rows) no expert is named by more than 32 rows, a bound that some block reaches.
All inputs are finite; a program needn't handle non-finite values.
Results may differ from a plain program's by a relative error of at most 0.018.
Values may be sent and summed in bfloat16 or wider, within the bound.
No kernel may reach another device: no remote copies, remote signals or barrier semaphores. Data moves between devices by JAX's collectives and lax.ppermute only.
A program may use at most 64 MiB of HBM per device.

v0:
```python
import jax
import jax.numpy as jnp
from jax import lax
from jax.sharding import PartitionSpec as P

D = 2048
H = 256
SH = 256


EPSILON = 1e-05
ROUTED_SCALE = 2.5


def in_one_piece(arrays, axis, split_dim, concat_dim, along):
    both = jnp.concatenate(arrays, axis=along)
    whole, at, outs = (
        lax.all_to_all(both, axis, split_axis=split_dim, concat_axis=concat_dim, tiled=True),
        0,
        [],
    )
    for a in arrays:
        outs.append(lax.slice_in_dim(whole, at, at + a.shape[along], axis=along))
        at += a.shape[along]
    return tuple(outs)


def side_by_side(arrays, axis, dim, along):
    ends, at = ([], 0)
    for a in arrays[:-1]:
        at += a.shape[along]
        ends.append(at)
    both = jnp.concatenate(arrays, axis=along)
    return tuple(jnp.split(lax.all_gather(both, axis, axis=dim, tiled=True), ends, axis=along))


def from_everyone(shard, axis):
    length = lax.axis_size(axis)
    return lax.all_to_all(
        jnp.broadcast_to(shard[None], (length, *shard.shape)), axis, 0, 0, tiled=True
    )


def over_copies(shard, axis):
    everything = from_everyone(shard, axis)
    return jnp.sum(everything, axis=0)


def packed_total(arrays, axis):
    ends = [0]
    for a in arrays:
        ends.append(ends[-1] + a.size)
    running = over_copies(jnp.concatenate([a.ravel() for a in arrays]), axis)
    return tuple((running[b:e].reshape(a.shape) for a, b, e in zip(arrays, ends, ends[1:])))


def over_copies_2(shard, axis):
    return from_everyone(shard, axis).astype(jnp.float32).sum(axis=0)


def together(arrays, axis):
    ends = [0]
    for a in arrays:
        ends.append(ends[-1] + a.size)
    running = lax.psum(jnp.concatenate([a.ravel() for a in arrays]), axis)
    return tuple((running[b:e].reshape(a.shape) for a, b, e in zip(arrays, ends, ends[1:])))


def on_device(
    tokens,
    routes,
    route_scores,
    norm_gain,
    expert_gate,
    expert_up,
    expert_down,
    shared_gate,
    shared_up,
    shared_down,
):
    gain_column = norm_gain[:, None]
    gate_rows, up_rows, down_rows = in_one_piece(
        (
            (expert_gate * gain_column[None]).astype(jnp.bfloat16),
            (expert_up * gain_column[None]).astype(jnp.bfloat16),
            expert_down.astype(jnp.bfloat16),
        ),
        "fs",
        0,
        1,
        2,
    )
    shared_gate_rows, shared_up_rows, shared_down_rows = side_by_side(
        (
            (shared_gate * gain_column).astype(jnp.bfloat16),
            (shared_up * gain_column).astype(jnp.bfloat16),
            shared_down.astype(jnp.bfloat16),
        ),
        "fs",
        0,
        1,
    )
    served_gate, served_up, served_down, common_gate, common_up, common_down = (
        lax.all_to_all(gate_rows[0], "tp", split_axis=0, concat_axis=1, tiled=True),
        lax.all_to_all(up_rows[0], "tp", split_axis=0, concat_axis=1, tiled=True),
        lax.all_to_all(down_rows[0], "tp", split_axis=0, concat_axis=1, tiled=True),
        lax.all_to_all(shared_gate_rows, "tp", split_axis=0, concat_axis=1, tiled=True),
        lax.all_to_all(shared_up_rows, "tp", split_axis=0, concat_axis=1, tiled=True),
        lax.all_to_all(shared_down_rows, "tp", split_axis=0, concat_axis=1, tiled=True),
    )
    values = tokens.astype(jnp.float32)
    feature_sum, square_sum = packed_total(
        (jnp.sum(values, axis=1), jnp.sum(values * values, axis=1)), "tp"
    )
    average = feature_sum / D
    variance = square_sum / D - average * average
    normed = ((values - average[:, None]) * lax.rsqrt(variance + EPSILON)[:, None]).astype(
        jnp.bfloat16
    )
    shared_gate_part = jnp.dot(normed, common_gate, preferred_element_type=jnp.float32) * D ** (
        -0.5
    )
    shared_up_part = jnp.dot(normed, common_up, preferred_element_type=jnp.float32) * D ** (-0.5)
    shared_gate_total, shared_up_total = (
        over_copies_2(shared_gate_part.astype(jnp.bfloat16), "tp").astype(jnp.float32),
        over_copies_2(shared_up_part.astype(jnp.bfloat16), "tp").astype(jnp.float32),
    )
    shared_hidden = (jax.nn.silu(shared_gate_total) * shared_up_total).astype(jnp.bfloat16)
    shared_part = jnp.einsum(
        "th,dh->td", shared_hidden, common_down, preferred_element_type=jnp.float32
    ) * SH ** (-0.5)
    tok_rows, top_count = routes.shape
    experts = expert_gate.shape[0]
    capacity = 2 * tok_rows * top_count // experts
    expert_ids = routes.reshape(-1)
    one_hot = (expert_ids[:, None] == jnp.arange(experts, dtype=jnp.int32)[None, :]).astype(
        jnp.int32
    )
    slot_rank = jnp.sum(jnp.cumsum(one_hot, axis=0) * one_hot, axis=1) - 1
    slot_index = expert_ids * capacity + slot_rank
    token_index = jnp.arange(expert_ids.shape[0], dtype=jnp.int32) // top_count
    slot_token = (
        jnp.full((experts * capacity,), tok_rows, jnp.int32).at[slot_index].set(token_index)
    )
    padded = jnp.concatenate([normed, jnp.zeros((1, normed.shape[1]), jnp.bfloat16)], axis=0)
    outgoing = padded[slot_token].reshape(experts, capacity, normed.shape[1])
    received = lax.all_to_all(outgoing, "fs", split_axis=0, concat_axis=0, tiled=True)
    gate_part = jnp.einsum(
        "scd,dh->sch", received, served_gate, preferred_element_type=jnp.float32
    ) * D ** (-0.5)
    up_part = jnp.einsum(
        "scd,dh->sch", received, served_up, preferred_element_type=jnp.float32
    ) * D ** (-0.5)
    gate_total, up_total = tuple(
        (
            part.astype(jnp.float32)
            for part in together(
                (gate_part.astype(jnp.bfloat16), up_part.astype(jnp.bfloat16)), "tp"
            )
        )
    )
    hidden = (jax.nn.silu(gate_total) * up_total).astype(jnp.bfloat16)
    expert_out = jnp.einsum(
        "sch,dh->scd", hidden, served_down, preferred_element_type=jnp.float32
    ) * H ** (-0.5)
    returned = lax.all_to_all(
        expert_out.astype(jnp.bfloat16), "fs", split_axis=0, concat_axis=0, tiled=True
    )
    picked = returned.reshape(experts * capacity, returned.shape[2])[slot_index]
    picked = picked.reshape(tok_rows, top_count, returned.shape[2]).astype(jnp.float32)
    mix_weight = route_scores / jnp.sum(route_scores, axis=1, keepdims=True) * ROUTED_SCALE
    routed_part = jnp.sum(picked * mix_weight[:, :, None], axis=1)
    mixture = (shared_part + routed_part).astype(jnp.bfloat16)
    return (
        served_gate[None],
        served_up[None],
        served_down[None],
        common_gate,
        common_up,
        common_down,
        mixture,
    )


def solution(mesh):
    in_specs = (
        P(("grp", "fs"), "tp"),
        P(("grp", "fs"), None),
        P(("grp", "fs"), None),
        P("fs"),
        P(None, "fs", "tp"),
        P(None, "fs", "tp"),
        P(None, "fs", "tp"),
        P("fs", "tp"),
        P("fs", "tp"),
        P("fs", "tp"),
    )
    out_specs = (
        P(("grp", "fs"), "tp", None),
        P(("grp", "fs"), "tp", None),
        P(("grp", "fs"), "tp", None),
        P(("grp", "tp"), None),
        P(("grp", "tp"), None),
        P(("grp", "tp"), None),
        P(("grp", "fs"), "tp"),
    )
    return jax.shard_map(
        on_device, mesh=mesh, in_specs=in_specs, out_specs=out_specs, check_vma=False
    )
```

profile of v0, /device:TPU:40, one launch (start us, length us, event | category | flops | bytes accessed | tf_op | source)
XLA Modules:
  0.0 762.4 jit_solution(9510454067890676347)
XLA Ops:
  7.2 1.1 convert_reduce_fusion.2
  8.3 0.6 broadcast_in_dim.19
  8.9 4.6 all-to-all-start.7
  13.5 1.3 convert_element_type.79
  14.8 1.5 multiply_convert_fusion.5
  16.4 1.5 pad_maximum_fusion.1
  17.9 0.9 all-to-all-done.7
  18.8 47.3 %all-to-all-start = ((bf16[64,32,192]{2,1,0:T(8,128)(2,1)}), bf16[64,32,192]{2,1,0:T(8,128)(2,1)S(1)}, u32[]{:S(2)}, u32[]{:S(2)}) async-start(bf16[64,32,192]{2,1,0:T(8,128)(2,1)} %pad_maximum_fusion.1), calls=%async_computation | async-start | bytes 2097152 | tf_op jit(solution)/shard_map/all_to_all | solution.py:18
  66.4 18.0 %reduce-window.6 = s32[64,8,128]{2,1,0:T(8,128)S(1)} reduce-window(s32[64,8,128]{2,1,0:T(8,128)S(1)} %fusion.10, s32[]{:T(128)} %constant.50.clone.1), window={size=1x1x128 pad=0_0x0_0x127_0}, to_apply=%region_5.6 | reduce-window | flops 8323072 | bytes 524292 | tf_op jit(solution)/shard_map/reduce-window
  85.3 4.3 scatter_custom_fusion
  89.7 85.6 %all-to-all-done = bf16[64,32,192]{2,1,0:T(8,128)(2,1)S(1)} async-done(((bf16[64,32,192]{2,1,0:T(8,128)(2,1)}), bf16[64,32,192]{2,1,0:T(8,128)(2,1)S(1)}, u32[]{:S(2)}, u32[]{:S(2)}) %all-to-all-start) | async-done | bytes 786464 | tf_op jit(solution)/shard_map/all_to_all | solution.py:18
  175.3 1.3 fusion.21
  176.6 0.9 copy.130
  177.5 3.9 all-to-all-start.1
  181.5 9.2 %gather_fusion = bf16[2048,512]{1,0:T(8,128)(2,1)} fusion(bf16[129,512]{1,0:T(8,128)(2,1)S(1)} %concatenate.18, s32[2048]{0:T(1024)S(1)} %fusion.12), kind=kCustom, calls=%fused_computation | custom fusion | bytes 4202496 | tf_op jit(solution)/shard_map/gather | solution.py:146
  190.7 6.7 all-to-all-start.10
  197.4 0.9 copy.132
  198.3 198.2 %all-to-all-done.10 = bf16[64,32,512]{2,1,0:T(8,128)(2,1)S(1)} async-done(((bf16[64,32,512]{2,1,0:T(8,128)(2,1)}), bf16[64,32,512]{2,1,0:T(8,128)(2,1)S(1)}, u32[]{:S(2)}, u32[]{:S(2)}) %all-to-all-start.10) | async-done | bytes 2097184 | tf_op jit(solution)/shard_map/all_to_all | solution.py:147
  396.5 4.8 all-to-all-start.2
  401.3 0.7 multiply_convert_fusion.3
  402.0 1.1 copy.182
  403.1 5.0 all-to-all-done.2
  408.1 1.7 multiply_convert_fusion.2
  409.8 1.1 copy.183
  410.8 1.4 pad_maximum_fusion
  412.4 0.6 copy-done.11
  413.2 55.6 %all_gather.3 = bf16[2048,192]{1,0:T(8,128)(2,1)S(1)} all-gather(bf16[32,192]{1,0:T(8,128)(2,1)S(1)} %pad_maximum_fusion.2), channel_id=1, replica_groups=mesh['grp'=2,'fs'=64,'tp'=4] {'fs'}, dimensions={0}, use_global_device_ids=true | all-gather | bytes 798720 | tf_op jit(solution)/shard_map/all_gather | solution.py:34
  468.8 0.3 fusion.20
  469.1 0.9 copy.138
  470.0 3.5 all-to-all-start.5
  473.5 0.9 copy.136
  474.4 9.7 %all-to-all-done.5 = bf16[4,512,64]{1,2,0:T(8,128)(2,1)S(1)} async-done(((bf16[4,512,64]{1,2,0:T(8,128)(2,1)}), bf16[4,512,64]{1,2,0:T(8,128)(2,1)S(1)}, u32[]{:S(2)}, u32[]{:S(2)}) %all-to-all-start.5) | async-done | bytes 262176 | tf_op jit(solution)/shard_map/all_to_all | solution.py:108
  484.1 3.5 all-to-all-start.4
  487.6 0.9 copy.140
  488.5 5.7 all-to-all-done.4
  494.3 3.5 all-to-all-start.6
  498.0 6.4 all-to-all-done.6
  504.4 0.8 broadcast_in_dim.21
  505.1 3.5 all-to-all-start.9
  508.9 0.9 copy.134
  509.8 5.4 all-to-all-done.9
  515.2 4.1 all-to-all-start.3
  519.4 3.1 slice_convert_fusion.1
  522.5 2.9 reshape.148
  525.4 1.6 reshape.149
  527.0 0.7 broadcast_in_dim.20
  527.7 4.7 all-to-all-start.8
  532.4 4.4 multiply_convert_fusion
  536.9 2.2 all-to-all-done.8
  539.1 0.7 copy-done.5
  539.8 10.2 %all-to-all-start.11 = ((bf16[64,32,512]{2,1,0:T(8,128)(2,1)}), bf16[64,32,512]{2,1,0:T(8,128)(2,1)S(1)}, u32[]{:S(2)}, u32[]{:S(2)}) async-start(bf16[64,32,512]{2,1,0:T(8,128)(2,1)} %multiply_convert_fusion), calls=%async_computation.11 | async-start | bytes 4194304 | tf_op jit(solution)/shard_map/all_to_all | solution.py:166
  550.1 0.7 copy.150
  550.8 0.8 copy.154
  551.7 0.8 copy.155
  552.5 0.8 copy.156
  553.4 0.7 convert_reduce_fusion
  554.0 1.6 convert_reduce_fusion.1
  555.7 0.8 copy.151
  556.5 1.8 copy.152
  558.3 1.8 copy.153
  560.1 189.0 %all-to-all-done.11 = bf16[64,32,512]{2,1,0:T(8,128)(2,1)S(1)} async-done(((bf16[64,32,512]{2,1,0:T(8,128)(2,1)}), bf16[64,32,512]{2,1,0:T(8,128)(2,1)S(1)}, u32[]{:S(2)}, u32[]{:S(2)}) %all-to-all-start.11) | async-done | bytes 2097184 | tf_op jit(solution)/shard_map/all_to_all | solution.py:166
  749.1 4.0 gather_fusion.1
  753.1 0.7 fusion
  753.8 1.8 fusion.2
  (62 shorter events, 2.1 us)
Async XLA Ops:
  7.2 7.6 %copy-start.2 = (f32[64,32,64]{2,1,0:T(8,128)S(1)}, f32[64,32,64]{2,1,0:T(8,128)}, u32[]{:S(2)}) copy-start(f32[64,32,64]{2,1,0:T(8,128)} %param.14) | copy-start | bytes 1572868
  8.9 9.9 %all-to-all-start.7 = ((f32[4,1,256]{2,1,0:T(1,128)}), f32[4,1,256]{2,1,0:T(1,128)S(1)}, u32[]{:S(2)}, u32[]{:S(2)}) async-start(f32[4,1,256]{2,1,0:T(1,128)} %broadcast_in_dim.19), calls=%async_computation.7 | async-start | bytes 8192 | tf_op jit(solution)/shard_map/all_to_all | solution.py:39
  16.4 49.8 %copy-start.10 = (s32[128,8]{0,1:T(8,128)S(1)}, s32[128,8]{0,1:T(8,128)}, u32[]{:S(2)}) copy-start(s32[128,8]{0,1:T(8,128)} %param.11) | copy-start | bytes 12292
  18.8 156.5 %all-to-all-start = ((bf16[64,32,192]{2,1,0:T(8,128)(2,1)}), bf16[64,32,192]{2,1,0:T(8,128)(2,1)S(1)}, u32[]{:S(2)}, u32[]{:S(2)}) async-start(bf16[64,32,192]{2,1,0:T(8,128)(2,1)} %pad_maximum_fusion.1), calls=%async_computation | async-start | bytes 2097152 | tf_op jit(solution)/shard_map/all_to_all | solution.py:18
  175.3 6.1 copy-start.6
  177.5 13.2 %all-to-all-start.1 = ((bf16[4,512,64]{1,2,0:T(8,128)(2,1)}), bf16[4,512,64]{1,2,0:T(8,128)(2,1)S(1)}, u32[]{:S(2)}, u32[]{:S(2)}) async-start(bf16[4,512,64]{1,2,0:T(8,128)(2,1)} %copy.130), calls=%async_computation.1 | async-start | bytes 524288 | tf_op jit(solution)/shard_map/all_to_all | solution.py:104
  190.7 6.7 copy-start.1
  190.7 205.8 %all-to-all-start.10 = ((bf16[64,32,512]{2,1,0:T(8,128)(2,1)}), bf16[64,32,512]{2,1,0:T(8,128)(2,1)S(1)}, u32[]{:S(2)}, u32[]{:S(2)}) async-start(bf16[64,32,512]{2,1,0:T(8,128)(2,1)} %bitcast.23), calls=%async_computation.10 | async-start | bytes 4194304 | tf_op jit(solution)/shard_map/all_to_all | solution.py:147
  396.5 11.6 %all-to-all-start.2 = ((bf16[4,512,64]{1,2,0:T(8,128)(2,1)}), bf16[4,512,64]{1,2,0:T(8,128)(2,1)}, u32[]{:S(2)}, u32[]{:S(2)}) async-start(bf16[4,512,64]{1,2,0:T(8,128)(2,1)} %copy.132), calls=%async_computation.2 | async-start | bytes 524288 | tf_op jit(solution)/shard_map/all_to_all | solution.py:105
  401.3 118.1 %all-reduce.3.cloned.1.call-start = ((), (), s32[]{:S(2)}) async-start(), calls=%async_computation.12 | async-start | bytes 4194304 | tf_op jit(solution)/shard_map/psum | solution.py:65
  412.3 0.7 copy-start.11
  412.3 0.7 copy-start.8
  412.3 0.7 copy-start.9
  412.3 0.7 copy-start.13
  470.0 14.1 %all-to-all-start.5 = ((bf16[4,512,64]{1,2,0:T(8,128)(2,1)}), bf16[4,512,64]{1,2,0:T(8,128)(2,1)S(1)}, u32[]{:S(2)}, u32[]{:S(2)}) async-start(bf16[4,512,64]{1,2,0:T(8,128)(2,1)} %copy.138), calls=%async_computation.5 | async-start | bytes 524288 | tf_op jit(solution)/shard_map/all_to_all | solution.py:108
  473.5 35.4 %copy-start = (bf16[1,2048,64]{2,1,0:T(8,128)(2,1)S(1)}, bf16[1,2048,64]{2,1,0:T(8,128)(2,1)}, u32[]{:S(2)}) copy-start(bf16[1,2048,64]{2,1,0:T(8,128)(2,1)} %get-tuple-element.49) | copy-start | bytes 786436
  484.1 10.1 %all-to-all-start.4 = ((bf16[4,512,64]{1,2,0:T(8,128)(2,1)}), bf16[4,512,64]{1,2,0:T(8,128)(2,1)S(1)}, u32[]{:S(2)}, u32[]{:S(2)}) async-start(bf16[4,512,64]{1,2,0:T(8,128)(2,1)} %copy.136), calls=%async_computation.4 | async-start | bytes 524288 | tf_op jit(solution)/shard_map/all_to_all | solution.py:107
  494.3 10.1 %all-to-all-start.6 = ((bf16[4,512,64]{1,2,0:T(8,128)(2,1)}), bf16[4,512,64]{1,2,0:T(8,128)(2,1)S(1)}, u32[]{:S(2)}, u32[]{:S(2)}) async-start(bf16[4,512,64]{1,2,0:T(8,128)(2,1)} %copy.140), calls=%async_computation.6 | async-start | bytes 524288 | tf_op jit(solution)/shard_map/all_to_all | solution.py:109
  504.4 48.2 %copy-start.3 = (bf16[4,512,64]{1,2,0:T(8,128)(2,1)}, bf16[4,512,64]{1,2,0:T(8,128)(2,1)S(1)}, u32[]{:S(2)}) copy-start(bf16[4,512,64]{1,2,0:T(8,128)(2,1)S(1)} %all-to-all-done.6) | copy-start | bytes 786436
  505.1 10.1 %all-to-all-start.9 = ((bf16[4,128,256]{2,1,0:T(8,128)(2,1)}), bf16[4,128,256]{2,1,0:T(8,128)(2,1)S(1)}, u32[]{:S(2)}, u32[]{:S(2)}) async-start(bf16[4,128,256]{2,1,0:T(8,128)(2,1)} %broadcast_in_dim.21), calls=%async_computation.9 | async-start | bytes 524288 | tf_op jit(solution)/shard_map/all_to_all | solution.py:39
  515.2 11.8 %all-to-all-start.3 = ((bf16[4,512,64]{1,2,0:T(8,128)(2,1)}), bf16[4,512,64]{1,2,0:T(8,128)(2,1)}, u32[]{:S(2)}, u32[]{:S(2)}) async-start(bf16[4,512,64]{1,2,0:T(8,128)(2,1)} %copy.134), calls=%async_computation.3 | async-start | bytes 524288 | tf_op jit(solution)/shard_map/all_to_all | solution.py:106
  527.7 11.4 %all-to-all-start.8 = ((bf16[4,128,256]{2,1,0:T(8,128)(2,1)}), bf16[4,128,256]{2,1,0:T(8,128)(2,1)S(1)}, u32[]{:S(2)}, u32[]{:S(2)}) async-start(bf16[4,128,256]{2,1,0:T(8,128)(2,1)} %broadcast_in_dim.20), calls=%async_computation.8 | async-start | bytes 524288 | tf_op jit(solution)/shard_map/all_to_all | solution.py:39
  536.9 13.2 %copy-start.12 = (f32[128,8]{0,1:T(8,128)S(1)}, f32[128,8]{0,1:T(8,128)}, u32[]{:S(2)}) copy-start(f32[128,8]{0,1:T(8,128)} %param.12) | copy-start | bytes 12292
  539.1 0.7 copy-start.5
  539.8 209.3 %all-to-all-start.11 = ((bf16[64,32,512]{2,1,0:T(8,128)(2,1)}), bf16[64,32,512]{2,1,0:T(8,128)(2,1)S(1)}, u32[]{:S(2)}, u32[]{:S(2)}) async-start(bf16[64,32,512]{2,1,0:T(8,128)(2,1)} %multiply_convert_fusion), calls=%async_computation.11 | async-start | bytes 4194304 | tf_op jit(solution)/shard_map/all_to_all | solution.py:166
  749.1 4.0 copy-start.7
  749.1 4.7 copy-start.4
Sparse Core Ops, SparseCore 0:
  412.5 73.4 all-reduce.2
where the time goes:
time: 764 us; the launch traced here: 762 us
  waiting for transfers between devices  508 us (66%)
  starting transfers between devices  100 us (13%)
  blocking collectives  55.6 us (7%)
  local copies, waits for them, and re-layouts  43.2 us (6%)
  other arithmetic  31.7 us (4%)
  between operations  14.4 us (2%)
  matrix products  9.11 us (1%)
    all_to_all x1, waiting for transfers between devices, on_device(): lax.all_to_all(outgoing, 'fs', split_axis=0, concat_axis=0, tiled=True)  198 us
    all_to_all x1, waiting for transfers between devices, on_device(): lax.all_to_all(expert_out.astype(jnp.bfloat16), 'fs', split_axis=0, conca...  189 us
    all_to_all x1, waiting for transfers between devices, in_one_piece(): lax.all_to_all(both, axis, split_axis=split_dim, concat_axis=concat_dim,...  85.6 us
    all_gather x1, blocking collectives, side_by_side(): lax.all_gather(both, axis, axis=dim, tiled=True)  55.6 us
    all_to_all x1, starting transfers between devices, in_one_piece(): lax.all_to_all(both, axis, split_axis=split_dim, concat_axis=concat_dim,...  47.3 us
    another operation x3, other arithmetic  18.2 us
  transfers between devices with their start and end apart: 13, of which 10 were waited for; matrix products, arithmetic and copies ran while one was open for 9% of the time, Pallas kernels for 0%

commit v1 on v0

v1 whole, which is shorter than its diff:
```python
import jax
import jax.numpy as jnp
from jax import lax
from jax.sharding import PartitionSpec as P

EPSILON = 1e-05
ROUTED_SCALE = 2.5
BF16 = jnp.bfloat16
F32 = jnp.float32


def gather_tp(shard):
    length = lax.axis_size("tp")
    return lax.all_to_all(
        jnp.broadcast_to(shard[None], (length, *shard.shape)), "tp", 0, 0, tiled=True
    )


def mm(a, b):
    return jnp.dot(a, b, preferred_element_type=F32)


def mm_t(a, b):
    return lax.dot_general(a, b, (((1,), (1,)), ((), ())), preferred_element_type=F32)


def unpack_gate_up(parts):
    n, rows, both = parts.shape
    h = both // 2
    gate = parts[:, :, :h].transpose(1, 0, 2).reshape(rows, n * h)
    up = parts[:, :, h:].transpose(1, 0, 2).reshape(rows, n * h)
    return gate, up


def unpack_down(parts):
    n, src, half, both = parts.shape
    h = both // 2
    return (
        parts.reshape(n, src, half, 2, h).transpose(1, 3, 2, 0, 4).reshape(src * half * 2, n * h)
    )


def pack_down(down):
    half = down.shape[-2] // 2
    return jnp.concatenate([down[..., :half, :], down[..., half:, :]], axis=-1)


def on_device(
    tokens,
    routes,
    route_scores,
    norm_gain,
    expert_gate,
    expert_up,
    expert_down,
    shared_gate,
    shared_up,
    shared_down,
):
    n_fs, n_tp = lax.axis_size("fs"), lax.axis_size("tp")
    fs, tp = lax.axis_index("fs"), lax.axis_index("tp")
    rings = [list(range(c, n_fs, 2)) for c in range(2)]
    swap = [(i, i ^ 1) for i in range(n_fs)]
    rows_dev, feats = tokens.shape
    sub = rows_dev // n_tp
    width = feats * n_tp
    experts = expert_gate.shape[0]
    gain = norm_gain[:, None]
    hid = expert_gate.shape[2] * n_tp
    shared_hid = shared_gate.shape[1] * n_tp

    mine = lax.all_to_all(tokens.reshape(n_tp, sub, feats), "tp", 0, 0, tiled=True)
    values = mine.astype(F32)
    average = jnp.sum(values, axis=(0, 2)) / width
    meansq = jnp.sum(values * values, axis=(0, 2)) / width
    scale = lax.rsqrt(meansq - average * average + EPSILON)
    normed = ((values - average[None, :, None]) * scale[None, :, None]).astype(BF16)

    my_routes = lax.dynamic_slice_in_dim(routes, tp * sub, sub, 0)
    my_scores = lax.dynamic_slice_in_dim(route_scores, tp * sub, sub, 0)
    mix = my_scores / jnp.sum(my_scores, axis=1, keepdims=True) * ROUTED_SCALE
    named = my_routes[:, :, None] == jnp.arange(experts, dtype=jnp.int32)
    dense = jnp.sum(jnp.where(named, mix[:, :, None], 0.0), axis=1)
    high = dense.astype(BF16)
    low = (dense - high.astype(F32)).astype(BF16)
    payload = jnp.concatenate([*[normed[i] for i in range(n_tp)], high, low], axis=1)
    with jax.named_scope("tok_ag"):
        everyone = lax.all_gather(payload, "fs", axis=0, tiled=True, axis_index_groups=rings)

    gate_up = jnp.concatenate(
        [(expert_gate * gain).astype(BF16), (expert_up * gain).astype(BF16)], axis=2
    )
    with jax.named_scope("w_gu"):
        gate_up = lax.all_to_all(gate_up, "fs", 0, 0, tiled=True)
        gate, up = unpack_gate_up(gather_tp(gate_up.reshape(width, -1)))
    with jax.named_scope("w_dn"):
        down = lax.all_to_all(pack_down(expert_down.astype(BF16)), "fs", 0, 0, tiled=True)
        down = unpack_down(gather_tp(down))
    own = jnp.concatenate([gate, up, down], axis=1)
    other = lax.ppermute(own, "fs", swap)

    rows = everyone[:, :width]
    weights = everyone[:, width:].astype(F32)
    lanes = jnp.arange(2 * experts, dtype=jnp.int32) % experts
    partial = 0.0
    for w, e in ((own, fs), (other, fs ^ 1)):
        both = mm(rows, w[:, : 2 * hid]) * width**-0.5
        share = jnp.sum(jnp.where(lanes == e, weights, 0.0), axis=1, keepdims=True)
        hidden = (jax.nn.silu(both[:, :hid]) * both[:, hid:] * (share * hid**-0.5)).astype(BF16)
        partial = partial + mm_t(hidden, w[:, 2 * hid :])
    partial = partial.astype(BF16)

    packed = jnp.concatenate(
        [
            jnp.concatenate(
                [(shared_gate * gain).astype(BF16), (shared_up * gain).astype(BF16)], axis=1
            ),
            pack_down(shared_down.astype(BF16)),
        ],
        axis=0,
    )
    partial, packed, normed = lax.optimization_barrier((partial, packed, normed))
    with jax.named_scope("rs"):
        routed = lax.psum_scatter(
            partial, "fs", scatter_dimension=0, tiled=True, axis_index_groups=rings
        )
    local_rows = norm_gain.shape[0]
    with jax.named_scope("shared"):
        common = gather_tp_rows(lax.all_gather(packed, "fs", axis=0), local_rows)
        common_gate, common_up, common_down = common
        back = lax.all_to_all(normed, "tp", 0, 0, tiled=True).reshape(rows_dev, feats)
        part = jnp.concatenate([mm(back, common_gate), mm(back, common_up)], axis=1)
        part = (part * width**-0.5).astype(BF16)
        total = gather_tp(part).astype(F32).sum(axis=0)
        shared_hidden = (
            jax.nn.silu(total[:, :shared_hid]) * total[:, shared_hid:]
        ).astype(BF16)
        shared_part = mm_t(shared_hidden, common_down) * shared_hid**-0.5

    served = lax.dynamic_slice_in_dim(own, tp * feats, feats, 0)
    home = routed.reshape(sub, n_tp, feats).transpose(1, 0, 2)
    home = lax.all_to_all(home, "tp", 0, 0, tiled=True).reshape(rows_dev, feats)
    mixture = (shared_part + home.astype(F32)).astype(BF16)
    return (
        served[None, :, :hid],
        served[None, :, hid : 2 * hid],
        served[None, :, 2 * hid :],
        common_gate,
        common_up,
        common_down,
        mixture,
    )


def gather_tp_rows(packed, local_rows):
    n_tp = lax.axis_size("tp")
    n_fs = packed.shape[0]
    per = n_fs // n_tp
    split = packed.reshape(n_tp, per, *packed.shape[1:])
    split = lax.all_to_all(split, "tp", 0, 0, tiled=True)
    both = split[:, :, :local_rows].reshape(n_tp, per * local_rows, -1)
    gate, up = unpack_gate_up(both)
    return gate, up, unpack_down(split[:, :, local_rows:])


def solution(mesh):
    in_specs = (
        P(("grp", "fs"), "tp"),
        P(("grp", "fs"), None),
        P(("grp", "fs"), None),
        P("fs"),
        P(None, "fs", "tp"),
        P(None, "fs", "tp"),
        P(None, "fs", "tp"),
        P("fs", "tp"),
        P("fs", "tp"),
        P("fs", "tp"),
    )
    out_specs = (
        P(("grp", "fs"), "tp", None),
        P(("grp", "fs"), "tp", None),
        P(("grp", "fs"), "tp", None),
        P(("grp", "tp"), None),
        P(("grp", "tp"), None),
        P(("grp", "tp"), None),
        P(("grp", "fs"), "tp"),
    )
    return jax.shard_map(
        on_device, mesh=mesh, in_specs=in_specs, out_specs=out_specs, check_vma=False
    )
```

time: 764 us -> 441 us (0.58)
  waiting for transfers between devices: 508 us -> 219 us
  other arithmetic: 31.7 us -> 8.01 us
  starting transfers between devices: 100 us -> 79.9 us
  blocking collectives: 55.6 us -> 72.6 us
  local copies, waits for them, and re-layouts: 43.2 us -> 29.4 us
    all_to_all x12 -> x8, waiting for transfers between devices: 508 us -> 141 us  [the longest x1 64.1 us: on_device(): gate_up = lax.all_to_all(gate_up, 'fs', 0, 0, tiled=True)]
    reduce_scatter x0 -> x1, waiting for transfers between devices: none -> 39.2 us  [on_device(): lax.psum_scatter(partial, 'fs', scatter_dimension=0, tiled=True, axis_ind...]
    all_gather x0 -> x1, waiting for transfers between devices: none -> 38.9 us  [on_device(): lax.all_gather(payload, 'fs', axis=0, tiled=True, axis_index_groups=rings)]
    all_to_all x12 -> x8, starting transfers between devices: 100 us -> 77.7 us  [the longest x1 47.3 us: on_device(): lax.all_to_all(pack_down(expert_down.astype(BF16)), 'fs', 0, 0, tiled=True)]
    another operation x3 -> x0, other arithmetic: 18.2 us -> none
    all_to_all x0 -> x1, blocking collectives: none -> 15.7 us  [gather_tp_rows(): split = lax.all_to_all(split, 'tp', 0, 0, tiled=True)]
    gather x2 -> x0, local copies, waits for them, and re-layouts: 13.1 us -> none  [the longest x1 9.18 us: on_device(): outgoing = padded[slot_token].reshape(experts, capacity, normed.shape[1])]
    reshape x0 -> x6, local copies, waits for them, and re-layouts: none -> 8.98 us  [the longest x5 7.42 us: unpack_down(): parts.reshape(n, src, half, 2, h).transpose(1, 3, 2, 0, 4)]
  transfers between devices with their start and end apart: 13 -> 11, of which waited for: 10 -> 9; matrix products, arithmetic and copies ran while one was open for 9% -> 10% of each run, Pallas kernels for 0% -> 0%
where the time goes in v1:
time: 441 us; the launch traced here: 440 us
  waiting for transfers between devices  219 us (50%)
  starting transfers between devices  79.9 us (18%)
  blocking collectives  72.6 us (16%)
  local copies, waits for them, and re-layouts  29.4 us (7%)
  matrix products  16.4 us (4%)
  between operations  14.5 us (3%)
  other arithmetic  8.01 us (2%)
    all_to_all x1, waiting for transfers between devices, on_device(): gate_up = lax.all_to_all(gate_up, 'fs', 0, 0, tiled=True)  64.1 us
    all_gather x1, blocking collectives, on_device(): common = gather_tp_rows(lax.all_gather(packed, 'fs', axis=0), local_rows)  56.9 us
    all_to_all x1, starting transfers between devices, on_device(): lax.all_to_all(pack_down(expert_down.astype(BF16)), 'fs', 0, 0, tiled=True)  47.3 us
    reduce_scatter x1, waiting for transfers between devices, on_device(): lax.psum_scatter(partial, 'fs', scatter_dimension=0, tiled=True, axis_ind...  39.2 us
    all_gather x1, waiting for transfers between devices, on_device(): lax.all_gather(payload, 'fs', axis=0, tiled=True, axis_index_groups=rings)  38.9 us
    all_to_all x1, waiting for transfers between devices, on_device(): lax.all_to_all(pack_down(expert_down.astype(BF16)), 'fs', 0, 0, tiled=True)  38.9 us
    all_to_all x3, waiting for transfers between devices, gather_tp(): lax.all_to_all(jnp.broadcast_to(shard[None], (length, *shard.shape)), 'tp...  22.9 us
    all_to_all x1, blocking collectives, gather_tp_rows(): split = lax.all_to_all(split, 'tp', 0, 0, tiled=True)  15.7 us
  transfers between devices with their start and end apart: 11, of which 9 were waited for; matrix products, arithmetic and copies ran while one was open for 10% of the time, Pallas kernels for 0%

profile of v1, /device:TPU:40, one launch (start us, length us, event | category | flops | bytes accessed | tf_op | source)
XLA Modules:
  0.0 439.7 jit_solution(9491800243353704792)
XLA Ops:
  7.2 4.7 %all-to-all-start.4 = ((bf16[4,32,512]{2,1,0:T(8,128)(2,1)}), bf16[4,32,512]{2,1,0:T(8,128)(2,1)S(1)}, u32[]{:S(2)}, u32[]{:S(2)}) async-start(bf16[4,32,512]{2,1,0:T(8,128)(2,1)} %bitcast.67), calls=%async_computation.4 | async-start | bytes 262144 | tf_op jit(solution)/shard_map/all_to_all | solution.py:72
  12.0 1.3 convert_element_type.69
  13.3 0.9 pad_maximum_fusion.2
  14.2 3.8 all-to-all-done.4
  17.9 47.3 %all-to-all-start.2 = ((bf16[64,16,128]{2,1,0:T(8,128)(2,1)}), bf16[64,16,128]{2,1,0:T(8,128)(2,1)S(1)}, u32[]{:S(2)}, u32[]{:S(2)}) async-start(bf16[64,16,128]{2,1,0:T(8,128)(2,1)} %pad_maximum_fusion.2), calls=%async_computation.2 | async-start | bytes 524288 | tf_op jit(solution)/shard_map/w_dn/all_to_all | solution.py:97
  65.3 0.1 dynamic-slice_reduce_fusion
  65.7 0.3 multiply_convert_fusion.1
  66.0 1.1 pad_maximum_fusion.1
  67.1 0.1 select_reduce_fusion
  67.2 0.1 convert_reduce_fusion.1
  67.4 0.8 fusion.35
  68.2 38.9 %all-to-all-done.2 = bf16[64,16,128]{2,1,0:T(8,128)(2,1)S(1)} async-done(((bf16[64,16,128]{2,1,0:T(8,128)(2,1)}), bf16[64,16,128]{2,1,0:T(8,128)(2,1)S(1)}, u32[]{:S(2)}, u32[]{:S(2)}) %all-to-all-start.2) | async-done | bytes 262176 | tf_op jit(solution)/shard_map/w_dn/all_to_all | solution.py:97
  107.0 6.5 %all-to-all-start = ((bf16[64,32,128]{2,1,0:T(8,128)(2,1)}), bf16[64,32,128]{2,1,0:T(8,128)(2,1)S(1)}, u32[]{:S(2)}, u32[]{:S(2)}) async-start(bf16[64,32,128]{2,1,0:T(8,128)(2,1)} %pad_maximum_fusion.1), calls=%async_computation | async-start | bytes 1048576 | tf_op jit(solution)/shard_map/w_gu/all_to_all | solution.py:94
  113.6 0.8 slice_bitcast_fusion.2
  114.4 0.7 concatenate.34
  115.2 64.1 %all-to-all-done = bf16[64,32,128]{2,1,0:T(8,128)(2,1)S(1)} async-done(((bf16[64,32,128]{2,1,0:T(8,128)(2,1)}), bf16[64,32,128]{2,1,0:T(8,128)(2,1)S(1)}, u32[]{:S(2)}, u32[]{:S(2)}) %all-to-all-start) | async-done | bytes 524320 | tf_op jit(solution)/shard_map/w_gu/all_to_all | solution.py:94
  179.3 1.2 broadcast_in_dim.63
  180.5 3.6 all-to-all-start.3
  184.1 0.2 copy.60
  184.3 12.6 %all-to-all-done.3 = bf16[4,64,16,128]{3,2,1,0:T(8,128)(2,1)S(1)} async-done(((bf16[4,64,16,128]{3,2,1,0:T(8,128)(2,1)}), bf16[4,64,16,128]{3,2,1,0:T(8,128)(2,1)S(1)}, u32[]{:S(2)}, u32[]{:S(2)}) %all-to-all-start.3) | async-done | bytes 1048608 | tf_op jit(solution)/shard_map/w_dn/all_to_all | solution.py:14
  197.0 1.7 broadcast_in_dim.62
  198.6 3.7 all-to-all-start.1
  202.4 1.9 reshape.102
  204.3 5.7 %copy.61 = bf16[64,2,16,4,64]{4,3,2,1,0:T(4,128)(2,1)} copy(bf16[64,2,16,4,64]{4,1,2,0,3:T(2,128)(2,1)} %bitcast.52) | data formatting | bytes 2097152 | tf_op jit(solution)/shard_map/w_dn/transpose | solution.py:39
  210.0 3.5 reshape.103
  213.5 1.4 copy.62
  214.9 10.3 %all-to-all-done.1 = bf16[4,2048,128]{1,2,0:T(8,128)(2,1)S(1)} async-done(((bf16[4,2048,128]{1,2,0:T(8,128)(2,1)}), bf16[4,2048,128]{1,2,0:T(8,128)(2,1)S(1)}, u32[]{:S(2)}, u32[]{:S(2)}) %all-to-all-start.1) | async-done | bytes 2097184 | tf_op jit(solution)/shard_map/w_gu/all_to_all | solution.py:14
  225.2 0.1 fusion.45
  225.4 1.4 copy-done.1
  226.9 1.8 pad_maximum_fusion
  228.7 2.1 collective-permute-start
  230.9 0.1 maximum_maximum_fusion
  231.0 38.9 %all-gather.3.cloned.1.call-done = bf16[1024,2176]{1,0:T(8,128)(2,1)} async-done(((bf16[32,2176]{1,0:T(8,128)(2,1)}), bf16[1024,2176]{1,0:T(8,128)(2,1)}) %all-gather.3.cloned.1.call-update) | async-done | bytes 4456464 | tf_op jit(solution)/shard_map/tok_ag/all_gather | solution.py:88
  269.9 1.2 fusion.26
  271.1 5.2 %fusion.13 = f32[1024,512]{1,0:T(8,128)S(1)} fusion(bf16[2048,256]{0,1:T(8,128)(2,1)} %bitcast.57, bf16[2048,256]{0,1:T(8,128)(2,1)} %bitcast.55, bf16[1024,2176]{1,0:T(8,128)(2,1)} %all-gather.3.cloned.1.call-done), kind=kOutput, calls=%fused_computation.11 | convolution fusion | flops 2152202240 | bytes 8388608 | tf_op jit(solution)/shard_map/dot_general | solution.py:20
  276.3 1.3 fusion.27
  277.6 0.9 copy-done.11
  278.6 4.0 fusion.8
  282.5 4.6 %add_convert_fusion = bf16[1024,2048]{1,0:T(8,128)(2,1)} fusion(f32[1024,2048]{1,0:T(8,128)S(1)} %fusion.27, bf16[2048,768]{0,1:T(8,128)(2,1)} %collective-permute-done, f32[1024,512]{1,0:T(8,128)S(1)} %fusion.8, f32[1024]{0:T(1024)S(1)} %broadcast_multiply_fusion), kind=kOutput, calls=%fused_computation | convolution fusion | flops 1079771136 | bytes 15732736 | tf_op jit(solution)/shard_map/dot_general | solution.py:24
  287.2 56.9 %all-gather = bf16[3072,128]{1,0:T(8,128)(2,1)S(1)} all-gather(bf16[48,128]{1,0:T(8,128)(2,1)S(1)} %maximum_maximum_fusion), channel_id=2, replica_groups=mesh['grp'=2,'fs'=64,'tp'=4] {'fs'}, dimensions={0}, use_global_device_ids=true | all-gather | bytes 798720 | tf_op jit(solution)/shard_map/shared/all_gather | solution.py:129
  344.1 15.7 %all_to_all.45 = bf16[4,16,48,128]{3,2,1,0:T(8,128)(2,1)S(1)} all-to-all(bf16[4,16,48,128]{3,2,1,0:T(8,128)(2,1)S(1)} %bitcast.58), channel_id=1, replica_groups=mesh['grp'=2,'fs'=64,'tp'=4] {'tp'}, dimensions={0} | all-to-all | bytes 1572864 | tf_op jit(solution)/shard_map/shared/all_to_all | solution.py:160
  359.8 3.4 all-to-all-start.6
  363.2 0.2 slice_bitcast_fusion
  363.5 0.2 copy.66
  363.7 0.2 copy.65
  363.9 5.2 %all-to-all-done.6 = bf16[4,32,512]{2,1,0:T(8,128)(2,1)S(1)} async-done(((bf16[4,32,512]{2,1,0:T(8,128)(2,1)}), bf16[4,32,512]{2,1,0:T(8,128)(2,1)S(1)}, u32[]{:S(2)}, u32[]{:S(2)}) %all-to-all-start.6) | async-done | bytes 131104 | tf_op jit(solution)/shard_map/shared/all_to_all | solution.py:131
  369.1 0.2 fusion.49
  369.3 0.2 fusion.48
  369.6 0.9 broadcast_in_dim.72
  370.5 3.6 all-to-all-start.7
  374.0 1.2 dynamic-slice_bitcast_fusion
  375.2 0.8 copy.71
  376.0 0.8 copy.70
  376.9 0.8 copy.69
  377.7 0.8 copy.73
  378.6 0.8 copy.72
  379.4 0.2 reshape.109
  379.7 0.4 copy.67
  380.1 0.3 reshape.110
  380.4 39.2 %reduce-scatter.2.cloned.1.call-done = bf16[32,2048]{1,0:T(8,128)(2,1)} async-done(((bf16[1024,2048]{1,0:T(8,128)(2,1)}), bf16[32,2048]{1,0:T(8,128)(2,1)}) %reduce-scatter.2.cloned.1.call-update) | async-done | bytes 131088 | tf_op jit(solution)/shard_map/rs/reduce_scatter | solution.py:124
  419.6 1.6 copy.76
  421.2 4.8 %all-to-all-start.8 = ((bf16[4,32,512]{2,1,0:T(8,128)(2,1)}), bf16[4,32,512]{2,1,0:T(8,128)(2,1)S(1)}, u32[]{:S(2)}, u32[]{:S(2)}) async-start(bf16[4,32,512]{2,1,0:T(8,128)(2,1)} %bitcast.51), calls=%async_computation.9 | async-start | bytes 262144 | tf_op jit(solution)/shard_map/all_to_all | solution.py:142
  426.1 5.9 %all-to-all-done.8 = bf16[4,32,512]{2,1,0:T(8,128)(2,1)S(1)} async-done(((bf16[4,32,512]{2,1,0:T(8,128)(2,1)}), bf16[4,32,512]{2,1,0:T(8,128)(2,1)S(1)}, u32[]{:S(2)}, u32[]{:S(2)}) %all-to-all-start.8) | async-done | bytes 131104 | tf_op jit(solution)/shard_map/all_to_all | solution.py:142
  432.0 0.9 fusion.19
  (47 shorter events, 0.9 us)
Async XLA Ops:
  7.2 58.2 %copy-start = (s32[128,8]{0,1:T(8,128)S(1)}, s32[128,8]{0,1:T(8,128)}, u32[]{:S(2)}) copy-start(s32[128,8]{0,1:T(8,128)} %param.11) | copy-start | bytes 12292
  7.2 58.1 %copy-start.10 = (f32[128,8]{0,1:T(8,128)S(1)}, f32[128,8]{0,1:T(8,128)}, u32[]{:S(2)}) copy-start(f32[128,8]{0,1:T(8,128)} %param.12) | copy-start | bytes 12292
  7.2 58.5 %copy-start.12 = (f32[32]{0:T(128)S(1)}, f32[32]{0:T(128)}, u32[]{:S(2)}) copy-start(f32[32]{0:T(128)} %param.13) | copy-start | bytes 388
  7.2 58.5 %copy-start.5 = (f32[64,32,64]{2,1,0:T(8,128)S(1)}, f32[64,32,64]{2,1,0:T(8,128)}, u32[]{:S(2)}) copy-start(f32[64,32,64]{2,1,0:T(8,128)} %param.15) | copy-start | bytes 1572868
  7.2 58.5 %copy-start.4 = (f32[64,32,64]{2,1,0:T(8,128)S(1)}, f32[64,32,64]{2,1,0:T(8,128)}, u32[]{:S(2)}) copy-start(f32[64,32,64]{2,1,0:T(8,128)} %param.14) | copy-start | bytes 1572868
  7.2 10.7 %all-to-all-start.4 = ((bf16[4,32,512]{2,1,0:T(8,128)(2,1)}), bf16[4,32,512]{2,1,0:T(8,128)(2,1)S(1)}, u32[]{:S(2)}, u32[]{:S(2)}) async-start(bf16[4,32,512]{2,1,0:T(8,128)(2,1)} %bitcast.67), calls=%async_computation.4 | async-start | bytes 262144 | tf_op jit(solution)/shard_map/all_to_all | solution.py:72
  17.9 89.1 %all-to-all-start.2 = ((bf16[64,16,128]{2,1,0:T(8,128)(2,1)}), bf16[64,16,128]{2,1,0:T(8,128)(2,1)S(1)}, u32[]{:S(2)}, u32[]{:S(2)}) async-start(bf16[64,16,128]{2,1,0:T(8,128)(2,1)} %pad_maximum_fusion.2), calls=%async_computation.2 | async-start | bytes 524288 | tf_op jit(solution)/shard_map/w_dn/all_to_all | solution.py:97
  107.0 72.3 %all-to-all-start = ((bf16[64,32,128]{2,1,0:T(8,128)(2,1)}), bf16[64,32,128]{2,1,0:T(8,128)(2,1)S(1)}, u32[]{:S(2)}, u32[]{:S(2)}) async-start(bf16[64,32,128]{2,1,0:T(8,128)(2,1)} %pad_maximum_fusion.1), calls=%async_computation | async-start | bytes 1048576 | tf_op jit(solution)/shard_map/w_gu/all_to_all | solution.py:94
  113.5 156.4 %all-gather.3.cloned.1.call-start = ((), (), s32[]{:S(2)}) async-start(), calls=%async_computation.10 | async-start | bytes 4595712 | tf_op jit(solution)/shard_map/tok_ag/all_gather | solution.py:88
  180.5 16.5 %all-to-all-start.3 = ((bf16[4,64,16,128]{3,2,1,0:T(8,128)(2,1)}), bf16[4,64,16,128]{3,2,1,0:T(8,128)(2,1)S(1)}, u32[]{:S(2)}, u32[]{:S(2)}) async-start(bf16[4,64,16,128]{3,2,1,0:T(8,128)(2,1)} %broadcast_in_dim.63), calls=%async_computation.3 | async-start | bytes 2097152 | tf_op jit(solution)/shard_map/w_dn/all_to_all | solution.py:14
  198.6 26.6 %all-to-all-start.1 = ((bf16[4,2048,128]{1,2,0:T(8,128)(2,1)}), bf16[4,2048,128]{1,2,0:T(8,128)(2,1)S(1)}, u32[]{:S(2)}, u32[]{:S(2)}) async-start(bf16[4,2048,128]{1,2,0:T(8,128)(2,1)} %broadcast_in_dim.62), calls=%async_computation.1 | async-start | bytes 4194304 | tf_op jit(solution)/shard_map/w_gu/all_to_all | solution.py:14
  202.3 217.3 %reduce-scatter.2.cloned.1.call-start = ((), (), s32[]{:S(2)}) async-start(), calls=%async_computation.11 | async-start | bytes 4325376 | tf_op jit(solution)/shard_map/rs/reduce_scatter | solution.py:124
  225.2 1.6 copy-start.1
  225.4 3.3 copy-start.2
  225.4 3.3 copy-start.3
  226.8 4.0 copy-start.9
  226.8 4.0 copy-start.7
  226.8 4.0 copy-start.8
  228.7 49.0 %collective-permute-start = (bf16[2048,768]{0,1:T(8,128)(2,1)}, bf16[2048,768]{0,1:T(8,128)(2,1)}, u32[]{:S(2)}, u32[]{:S(2)}) collective-permute-start(bf16[2048,768]{0,1:T(8,128)(2,1)} %pad_maximum_fusion), channel_id=1, source_target_pairs={{0,4},{4,0},{8,12},{12,8},{16,20},{20,16},{24,28},{28,24},{32,36},... | collective-permute-start | bytes 9437192 | tf_op jit(solution)/shard_map/ppermute | solution.py:100
  276.3 2.3 copy-start.11
  359.8 9.3 %all-to-all-start.6 = ((bf16[4,32,512]{2,1,0:T(8,128)(2,1)}), bf16[4,32,512]{2,1,0:T(8,128)(2,1)S(1)}, u32[]{:S(2)}, u32[]{:S(2)}) async-start(bf16[4,32,512]{2,1,0:T(8,128)(2,1)} %fusion.35), calls=%async_computation.6 | async-start | bytes 262144 | tf_op jit(solution)/shard_map/shared/all_to_all | solution.py:131
  370.5 50.7 %all-to-all-start.7 = ((bf16[4,128,512]{2,1,0:T(8,128)(2,1)}), bf16[4,128,512]{2,1,0:T(8,128)(2,1)S(1)}, u32[]{:S(2)}, u32[]{:S(2)}) async-start(bf16[4,128,512]{2,1,0:T(8,128)(2,1)} %broadcast_in_dim.72), calls=%async_computation.7 | async-start | bytes 1048576 | tf_op jit(solution)/shard_map/shared/all_to_all | solution.py:14
  380.4 52.4 %copy-start.6 = (bf16[512,256]{1,0:T(8,128)(2,1)}, bf16[512,256]{1,0:T(8,128)(2,1)S(1)}, u32[]{:S(2)}) copy-start(bf16[512,256]{1,0:T(8,128)(2,1)S(1)} %reshape.110) | copy-start | bytes 786436
  421.2 10.8 %all-to-all-start.8 = ((bf16[4,32,512]{2,1,0:T(8,128)(2,1)}), bf16[4,32,512]{2,1,0:T(8,128)(2,1)S(1)}, u32[]{:S(2)}, u32[]{:S(2)}) async-start(bf16[4,32,512]{2,1,0:T(8,128)(2,1)} %bitcast.51), calls=%async_computation.9 | async-start | bytes 262144 | tf_op jit(solution)/shard_map/all_to_all | solution.py:142
Sparse Core Ops, SparseCore 0:
  117.0 152.8 all-gather.2
  287.3 132.2 reduce-scatter.1

commit v2 on v1

--- a/solution.py
+++ b/solution.py
@@ -9,10 +9,10 @@
 F32 = jnp.float32
 
 
-def gather_tp(shard):
-    length = lax.axis_size("tp")
+def broadcast_gather(shard, axis):
+    length = lax.axis_size(axis)
     return lax.all_to_all(
-        jnp.broadcast_to(shard[None], (length, *shard.shape)), "tp", 0, 0, tiled=True
+        jnp.broadcast_to(shard[None], (length, *shard.shape)), axis, 0, 0, tiled=True
     )
 
 
@@ -24,20 +24,19 @@
     return lax.dot_general(a, b, (((1,), (1,)), ((), ())), preferred_element_type=F32)
 
 
-def unpack_gate_up(parts):
-    n, rows, both = parts.shape
+def unpack(parts, rows):
+    n, src, _, both = parts.shape
     h = both // 2
-    gate = parts[:, :, :h].transpose(1, 0, 2).reshape(rows, n * h)
-    up = parts[:, :, h:].transpose(1, 0, 2).reshape(rows, n * h)
-    return gate, up
+    top, low = parts[:, :, :rows], parts[:, :, rows:]
+    low = jnp.concatenate([low[..., :h], low[..., h:]], axis=2)
+    return tuple(
+        jnp.concatenate([a[i].reshape(src * rows, h) for i in range(n)], axis=1)
+        for a in (top[..., :h], top[..., h:], low)
+    )
 
 
-def unpack_down(parts):
-    n, src, half, both = parts.shape
-    h = both // 2
-    return (
-        parts.reshape(n, src, half, 2, h).transpose(1, 3, 2, 0, 4).reshape(src * half * 2, n * h)
-    )
+def pack(gate, up, down):
+    return jnp.concatenate([jnp.concatenate([gate, up], axis=-1), pack_down(down)], axis=-2)
 
 
 def pack_down(down):
@@ -84,18 +83,24 @@
     high = dense.astype(BF16)
     low = (dense - high.astype(F32)).astype(BF16)
     payload = jnp.concatenate([*[normed[i] for i in range(n_tp)], high, low], axis=1)
+
+    local_rows = norm_gain.shape[0]
+    packed = pack(
+        (expert_gate * gain).astype(BF16),
+        (expert_up * gain).astype(BF16),
+        expert_down.astype(BF16),
+    )
+    n_grp = lax.axis_size("grp")
+    cut = packed.shape[1] // n_grp
+    piece = lax.dynamic_slice_in_dim(packed, lax.axis_index("grp") * cut, cut, 1)
+    payload, piece = lax.optimization_barrier((payload, piece))
     with jax.named_scope("tok_ag"):
         everyone = lax.all_gather(payload, "fs", axis=0, tiled=True, axis_index_groups=rings)
-
-    gate_up = jnp.concatenate(
-        [(expert_gate * gain).astype(BF16), (expert_up * gain).astype(BF16)], axis=2
-    )
-    with jax.named_scope("w_gu"):
-        gate_up = lax.all_to_all(gate_up, "fs", 0, 0, tiled=True)
-        gate, up = unpack_gate_up(gather_tp(gate_up.reshape(width, -1)))
-    with jax.named_scope("w_dn"):
-        down = lax.all_to_all(pack_down(expert_down.astype(BF16)), "fs", 0, 0, tiled=True)
-        down = unpack_down(gather_tp(down))
+    with jax.named_scope("weights"):
+        piece = lax.all_to_all(piece, "fs", 0, 0, tiled=True)
+        pieces = broadcast_gather(piece, "grp")
+        column = jnp.concatenate([pieces[i] for i in range(n_grp)], axis=1)
+        gate, up, down = unpack(broadcast_gather(column, "tp"), local_rows)
     own = jnp.concatenate([gate, up, down], axis=1)
     other = lax.ppermute(own, "fs", swap)
 
@@ -110,28 +115,25 @@
         partial = partial + mm_t(hidden, w[:, 2 * hid :])
     partial = partial.astype(BF16)
 
-    packed = jnp.concatenate(
-        [
-            jnp.concatenate(
-                [(shared_gate * gain).astype(BF16), (shared_up * gain).astype(BF16)], axis=1
-            ),
-            pack_down(shared_down.astype(BF16)),
-        ],
-        axis=0,
+    packed = pack(
+        (shared_gate * gain).astype(BF16),
+        (shared_up * gain).astype(BF16),
+        shared_down.astype(BF16),
     )
     partial, packed, normed = lax.optimization_barrier((partial, packed, normed))
     with jax.named_scope("rs"):
         routed = lax.psum_scatter(
             partial, "fs", scatter_dimension=0, tiled=True, axis_index_groups=rings
         )
-    local_rows = norm_gain.shape[0]
     with jax.named_scope("shared"):
-        common = gather_tp_rows(lax.all_gather(packed, "fs", axis=0), local_rows)
-        common_gate, common_up, common_down = common
+        common = lax.all_gather(packed, "fs", axis=0)
+        common = common.reshape(n_tp, n_fs // n_tp, *common.shape[1:])
+        common = lax.all_to_all(common, "tp", 0, 0, tiled=True)
+        common_gate, common_up, common_down = unpack(common, local_rows)
         back = lax.all_to_all(normed, "tp", 0, 0, tiled=True).reshape(rows_dev, feats)
         part = jnp.concatenate([mm(back, common_gate), mm(back, common_up)], axis=1)
         part = (part * width**-0.5).astype(BF16)
-        total = gather_tp(part).astype(F32).sum(axis=0)
+        total = broadcast_gather(part, "tp").astype(F32).sum(axis=0)
         shared_hidden = (
             jax.nn.silu(total[:, :shared_hid]) * total[:, shared_hid:]
         ).astype(BF16)
@@ -150,17 +152,6 @@
         common_down,
         mixture,
     )
-
-
-def gather_tp_rows(packed, local_rows):
-    n_tp = lax.axis_size("tp")
-    n_fs = packed.shape[0]
-    per = n_fs // n_tp
-    split = packed.reshape(n_tp, per, *packed.shape[1:])
-    split = lax.all_to_all(split, "tp", 0, 0, tiled=True)
-    both = split[:, :, :local_rows].reshape(n_tp, per * local_rows, -1)
-    gate, up = unpack_gate_up(both)
-    return gate, up, unpack_down(split[:, :, local_rows:])
 
 
 def solution(mesh):

time: 441 us -> 382 us (0.87)
  blocking collectives: 72.6 us -> 215 us
  waiting for transfers between devices: 219 us -> 80 us
  starting transfers between devices: 79.9 us -> 21.1 us
  local copies, waits for them, and re-layouts: 29.4 us -> 23.9 us
    all_to_all x1 -> x3, blocking collectives: 15.7 us -> 153 us  [the longest x1 104 us: on_device(): piece = lax.all_to_all(piece, 'fs', 0, 0, tiled=True)]
    all_to_all x5 -> x2, waiting for transfers between devices: 126 us -> 10.8 us  [the longest x1 10.8 us: on_device(): common = lax.all_to_all(common, 'tp', 0, 0, tiled=True)]
    all_to_all x5 -> x2, starting transfers between devices: 64.7 us -> 7.29 us  [the longest x1 3.73 us: on_device(): common = lax.all_to_all(common, 'tp', 0, 0, tiled=True)]
    all_gather x1, waiting for transfers between devices: 38.9 us -> 15.7 us  [on_device(): lax.all_gather(payload, 'fs', axis=0, tiled=True, axis_index_groups=rings)]
    concatenate x0 -> x2, local copies, waits for them, and re-layouts: none -> 13.5 us  [on_device(): own = jnp.concatenate([gate, up, down], axis=1)]
    reshape x5 -> x0, local copies, waits for them, and re-layouts: 7.42 us -> none  [unpack_down(): parts.reshape(n, src, half, 2, h).transpose(1, 3, 2, 0, 4)]
    transpose x5 -> x0, local copies, waits for them, and re-layouts: 6.72 us -> none  [the longest x2 6.08 us: unpack_down(): parts.reshape(n, src, half, 2, h).transpose(1, 3, 2, 0, 4)]
    unnamed x31 -> x34, local copies, waits for them, and re-layouts: 6.62 us -> 0.08 us
  transfers between devices with their start and end apart: 11 -> 8, of which waited for: 9 -> 6; matrix products, arithmetic and copies ran while one was open for 10% -> 10% of each run, Pallas kernels for 0% -> 0%
where the time goes in v2:
time: 382 us; the launch traced here: 380 us
  blocking collectives  215 us (56%)
  waiting for transfers between devices  80 us (21%)
  local copies, waits for them, and re-layouts  23.9 us (6%)
  starting transfers between devices  21.1 us (6%)
  matrix products  16.7 us (4%)
  between operations  14.5 us (4%)
  other arithmetic  8.76 us (2%)
    all_to_all x1, blocking collectives, on_device(): piece = lax.all_to_all(piece, 'fs', 0, 0, tiled=True)  104 us
    all_gather x1, blocking collectives, on_device(): common = lax.all_gather(packed, 'fs', axis=0)  61.6 us
    all_to_all x2, blocking collectives, broadcast_gather(): lax.all_to_all(jnp.broadcast_to(shard[None], (length, *shard.shape)), axi...  49.8 us
    reduce_scatter x1, waiting for transfers between devices, on_device(): lax.psum_scatter(partial, 'fs', scatter_dimension=0, tiled=True, axis_ind...  40.6 us
    all_gather x1, waiting for transfers between devices, on_device(): lax.all_gather(payload, 'fs', axis=0, tiled=True, axis_index_groups=rings)  15.7 us
    concatenate x2, local copies, waits for them, and re-layouts, on_device(): own = jnp.concatenate([gate, up, down], axis=1)  13.5 us
    all_to_all x1, waiting for transfers between devices, on_device(): common = lax.all_to_all(common, 'tp', 0, 0, tiled=True)  10.8 us
    dot_general x4, matrix products, mm(): return jnp.dot(a, b, preferred_element_type=F32)  9.62 us
  transfers between devices with their start and end apart: 8, of which 6 were waited for; matrix products, arithmetic and copies ran while one was open for 10% of the time, Pallas kernels for 0%

profile of v2, /device:TPU:40, one launch (start us, length us, event | category | flops | bytes accessed | tf_op | source)
XLA Modules:
  0.0 379.9 jit_solution(14263448494962802517)
XLA Ops:
  7.2 0.0 copy-start
  7.2 4.7 %all-to-all-start = ((bf16[4,32,512]{2,1,0:T(8,128)(2,1)}), bf16[4,32,512]{2,1,0:T(8,128)(2,1)S(1)}, u32[]{:S(2)}, u32[]{:S(2)}) async-start(bf16[4,32,512]{2,1,0:T(8,128)(2,1)} %bitcast.98), calls=%async_computation | async-start | bytes 262144 | tf_op jit(solution)/shard_map/all_to_all | solution.py:71
  12.0 0.8 dynamic-slice_reduce_fusion
  12.7 0.8 divide_multiply_fusion
  13.5 0.1 constant_dynamic-slice_fusion
  13.6 0.1 copy.23
  13.6 0.1 copy.24
  13.7 0.1 select_reduce_fusion
  13.9 1.3 convert_element_type.74
  15.3 0.3 multiply_convert_fusion
  15.6 0.6 fusion.40
  16.2 1.7 all-to-all-done
  17.9 0.1 convert_reduce_fusion.1
  18.1 0.8 fusion.43
  18.8 0.8 slice_bitcast_fusion.2
  19.7 0.7 concatenate.56
  20.4 0.1 all-gather.3.cloned.1.call-update
  20.5 0.1 reduce-scatter.2.cloned.1.call-start
  20.5 103.5 %all_to_all.40 = bf16[64,24,128]{2,1,0:T(8,128)(2,1)S(1)} all-to-all(bf16[64,24,128]{2,1,0:T(8,128)(2,1)S(1)} %fusion.40), channel_id=1, replica_groups=mesh['grp'=2,'fs'=64,'tp'=4] {'fs'}, dimensions={0} | all-to-all | bytes 786432 | tf_op jit(solution)/shard_map/weights/all_to_all | solution.py:100
  124.1 0.1 broadcast_in_dim.62
  124.2 11.0 %all_to_all.41 = bf16[2,64,24,128]{3,2,1,0:T(8,128)(2,1)S(1)} all-to-all(bf16[2,64,24,128]{3,2,1,0:T(8,128)(2,1)S(1)} %broadcast_in_dim.62), channel_id=1, replica_groups=mesh['grp'=2,'fs'=64,'tp'=4] {'grp'}, dimensions={0} | all-to-all | bytes 1572864 | tf_op jit(solution)/shard_map/weights/all_to_all | solution.py:14
  135.2 0.1 slice_bitcast_fusion.1
  135.3 0.1 pad_maximum_fusion
  135.4 0.4 broadcast_in_dim.63
  135.8 38.7 %all_to_all.42 = bf16[4,64,48,128]{3,2,1,0:T(8,128)(2,1)S(1)} all-to-all(bf16[4,64,48,128]{3,2,1,0:T(8,128)(2,1)S(1)} %broadcast_in_dim.63), channel_id=1, replica_groups=mesh['grp'=2,'fs'=64,'tp'=4] {'tp'}, dimensions={0} | all-to-all | bytes 6291456 | tf_op jit(solution)/shard_map/weights/all_to_all | solution.py:14
  174.5 0.5 fusion.56
  175.0 1.6 pad_maximum_fusion.1
  176.6 2.6 fusion.57
  179.2 7.0 %concatenate.62 = bf16[2048,768]{1,0:T(8,128)(2,1)S(1)} concatenate(bf16[2048,64]{1,0:T(8,128)(2,1)} %bitcast.74, bf16[2048,64]{1,0:T(8,128)(2,1)} %bitcast.72, bf16[2048,64]{1,0:T(8,128)(2,1)} %bitcast.70, bf16[2048,64]{1,0:T(8,128)(2,1)} %bitcast.68, bf16[2048,64]{1,0:T(8,128)(2,1)} %bitcast.66, bf16[2048,64]{1,0:T(8,128)(2,1)} %bitcast.64, bf16[2048,64]{1,0:T(8,128)(2,1)} %bitcast.62, ...), dimensions={1} | concatenate | bytes 6291456 | tf_op jit(solution)/shard_map/concatenate | solution.py:104
  186.2 2.1 collective-permute-start
  188.4 0.1 multiply_convert_fusion.3
  188.5 0.1 maximum_maximum_fusion
  188.6 6.5 %concatenate.63 = bf16[2048,512]{1,0:T(8,128)(2,1)} concatenate(bf16[2048,64]{1,0:T(8,128)(2,1)} %bitcast.75, bf16[2048,64]{1,0:T(8,128)(2,1)} %bitcast.73, bf16[2048,64]{1,0:T(8,128)(2,1)} %bitcast.71, bf16[2048,64]{1,0:T(8,128)(2,1)} %bitcast.69, bf16[2048,64]{1,0:T(8,128)(2,1)} %bitcast.67, bf16[2048,64]{1,0:T(8,128)(2,1)} %bitcast.65, bf16[2048,64]{1,0:T(8,128)(2,1)} %bitcast.63, ...), dimensions={1} | concatenate | bytes 4194304 | tf_op jit(solution)/shard_map/concatenate | solution.py:104
  195.1 15.7 %all-gather.3.cloned.1.call-done = bf16[1024,2176]{1,0:T(8,128)(2,1)} async-done(((bf16[32,2176]{1,0:T(8,128)(2,1)}), bf16[1024,2176]{1,0:T(8,128)(2,1)}) %all-gather.3.cloned.1.call-update) | async-done | bytes 4456464 | tf_op jit(solution)/shard_map/tok_ag/all_gather | solution.py:98
  210.7 1.3 fusion.29
  212.1 5.3 %fusion.5 = f32[1024,512]{1,0:T(8,128)S(1)} fusion(bf16[2048,512]{1,0:T(8,128)(2,1)} %concatenate.63, bf16[1024,2176]{1,0:T(8,128)(2,1)} %all-gather.3.cloned.1.call-done), kind=kOutput, calls=%fused_computation.12 | convolution fusion | flops 2148007936 | bytes 8388608 | tf_op jit(solution)/shard_map/dot_general | solution.py:20
  217.5 1.6 fusion.20
  219.2 3.9 %fusion.8 = f32[1024,512]{1,0:T(8,128)S(1)} fusion(bf16[2048,768]{1,0:T(8,128)(2,1)} %collective-permute-done, bf16[1024,2176]{1,0:T(8,128)(2,1)S(1)} %bitcast.102), kind=kOutput, calls=%fused_computation.13 | convolution fusion | flops 2148007936 | bytes 8388608 | tf_op jit(solution)/shard_map/dot_general | solution.py:20
  223.1 4.6 %add_convert_fusion = bf16[1024,2048]{1,0:T(8,128)(2,1)} fusion(f32[1024,2048]{1,0:T(8,128)S(1)} %fusion.20, bf16[2048,768]{1,0:T(8,128)(2,1)} %collective-permute-done, f32[1024,512]{1,0:T(8,128)S(1)} %fusion.8, f32[1024]{0:T(1024)S(1)} %broadcast_multiply_fusion), kind=kOutput, calls=%fused_computation | convolution fusion | flops 1079771136 | bytes 15732736 | tf_op jit(solution)/shard_map/dot_general | solution.py:24
  227.7 0.1 reduce-scatter.2.cloned.1.call-update
  227.8 61.6 %all-gather = bf16[3072,128]{1,0:T(8,128)(2,1)} all-gather(bf16[48,128]{1,0:T(8,128)(2,1)S(1)} %maximum_maximum_fusion), channel_id=2, replica_groups=mesh['grp'=2,'fs'=64,'tp'=4] {'fs'}, dimensions={0}, use_global_device_ids=true | all-gather | bytes 798720 | tf_op jit(solution)/shard_map/shared/all_gather | solution.py:129
  289.4 3.7 all-to-all-start.4
  293.1 2.0 dynamic-slice_bitcast_fusion
  295.1 10.8 %all-to-all-done.4 = bf16[4,16,48,128]{3,2,1,0:T(8,128)(2,1)S(1)} async-done(((bf16[4,16,48,128]{3,2,1,0:T(8,128)(2,1)}), bf16[4,16,48,128]{3,2,1,0:T(8,128)(2,1)S(1)}, u32[]{:S(2)}, u32[]{:S(2)}) %all-to-all-start.4) | async-done | bytes 786464 | tf_op jit(solution)/shard_map/shared/all_to_all | solution.py:131
  305.9 3.4 all-to-all-start.5
  309.4 0.2 fusion.59
  309.6 0.2 pad_maximum_fusion.3
  309.8 0.0 copy-start.6
  309.8 0.2 pad_maximum_fusion.2
  310.0 5.2 %all-to-all-done.5 = bf16[4,32,512]{2,1,0:T(8,128)(2,1)S(1)} async-done(((bf16[4,32,512]{2,1,0:T(8,128)(2,1)}), bf16[4,32,512]{2,1,0:T(8,128)(2,1)S(1)}, u32[]{:S(2)}, u32[]{:S(2)}) %all-to-all-start.5) | async-done | bytes 131104 | tf_op jit(solution)/shard_map/shared/all_to_all | solution.py:133
  315.2 0.2 fusion.63
  315.4 0.2 fusion.62
  315.7 0.9 broadcast_in_dim.70
  316.5 3.6 all-to-all-start.6
  320.1 0.1 fusion.58
  320.3 0.1 fusion.47
  320.4 0.2 pad_maximum_fusion.4
  320.6 0.0 copy-start.10
  320.6 40.6 %reduce-scatter.2.cloned.1.call-done = bf16[32,2048]{1,0:T(8,128)(2,1)} async-done(((bf16[1024,2048]{1,0:T(8,128)(2,1)}), bf16[32,2048]{1,0:T(8,128)(2,1)}) %reduce-scatter.2.cloned.1.call-update) | async-done | bytes 131088 | tf_op jit(solution)/shard_map/rs/reduce_scatter | solution.py:125
  361.2 1.6 copy.28
  362.7 3.5 all-to-all-start.7
  366.2 0.1 convert_reduce_fusion
  366.3 5.9 %all-to-all-done.7 = bf16[4,32,512]{2,1,0:T(8,128)(2,1)S(1)} async-done(((bf16[4,32,512]{2,1,0:T(8,128)(2,1)}), bf16[4,32,512]{2,1,0:T(8,128)(2,1)S(1)}, u32[]{:S(2)}, u32[]{:S(2)}) %all-to-all-start.7) | async-done | bytes 131104 | tf_op jit(solution)/shard_map/all_to_all | solution.py:144
  372.2 0.9 fusion.14
  (44 shorter events, 0.2 us)
Async XLA Ops:
  7.2 6.3 %copy-start = (s32[128,8]{0,1:T(8,128)S(1)}, s32[128,8]{0,1:T(8,128)}, u32[]{:S(2)}) copy-start(s32[128,8]{0,1:T(8,128)} %param.11) | copy-start | bytes 12292
  7.2 8.0 %copy-start.14 = (f32[32]{0:T(128)S(1)}, f32[32]{0:T(128)}, u32[]{:S(2)}) copy-start(f32[32]{0:T(128)} %param.13) | copy-start | bytes 388
  7.2 8.0 %copy-start.8 = (f32[64,32,64]{2,1,0:T(8,128)S(1)}, f32[64,32,64]{2,1,0:T(8,128)}, u32[]{:S(2)}) copy-start(f32[64,32,64]{2,1,0:T(8,128)} %param.15) | copy-start | bytes 1572868
  7.2 8.0 %copy-start.9 = (f32[64,32,64]{2,1,0:T(8,128)S(1)}, f32[64,32,64]{2,1,0:T(8,128)}, u32[]{:S(2)}) copy-start(f32[64,32,64]{2,1,0:T(8,128)} %param.14) | copy-start | bytes 1572868
  7.2 10.7 %all-to-all-start = ((bf16[4,32,512]{2,1,0:T(8,128)(2,1)}), bf16[4,32,512]{2,1,0:T(8,128)(2,1)S(1)}, u32[]{:S(2)}, u32[]{:S(2)}) async-start(bf16[4,32,512]{2,1,0:T(8,128)(2,1)} %bitcast.98), calls=%async_computation | async-start | bytes 262144 | tf_op jit(solution)/shard_map/all_to_all | solution.py:71
  11.9 198.8 %all-gather.3.cloned.1.call-start = ((), (), s32[]{:S(2)}) async-start(), calls=%async_computation.9 | async-start | bytes 4595712 | tf_op jit(solution)/shard_map/tok_ag/all_gather | solution.py:98
  20.5 340.7 %reduce-scatter.2.cloned.1.call-start = ((), (), s32[]{:S(2)}) async-start(), calls=%async_computation.10 | async-start | bytes 4325376 | tf_op jit(solution)/shard_map/rs/reduce_scatter | solution.py:125
  179.2 9.2 %copy-start.13 = (f32[32,64]{1,0:T(8,128)S(1)}, f32[32,64]{1,0:T(8,128)}, u32[]{:S(2)}) copy-start(f32[32,64]{1,0:T(8,128)} %param.19) | copy-start | bytes 24580
  179.2 9.2 %copy-start.11 = (f32[32,64]{1,0:T(8,128)S(1)}, f32[32,64]{1,0:T(8,128)}, u32[]{:S(2)}) copy-start(f32[32,64]{1,0:T(8,128)} %param.17) | copy-start | bytes 24580
  179.2 9.2 %copy-start.12 = (f32[32,64]{1,0:T(8,128)S(1)}, f32[32,64]{1,0:T(8,128)}, u32[]{:S(2)}) copy-start(f32[32,64]{1,0:T(8,128)} %param.18) | copy-start | bytes 24580
  186.2 8.9 %copy-start.1 = (bf16[2048,768]{1,0:T(8,128)(2,1)}, bf16[2048,768]{1,0:T(8,128)(2,1)S(1)}, u32[]{:S(2)}) copy-start(bf16[2048,768]{1,0:T(8,128)(2,1)S(1)} %concatenate.62) | copy-start | bytes 9437188
  186.2 32.9 %collective-permute-start = (bf16[2048,768]{1,0:T(8,128)(2,1)S(1)}, bf16[2048,768]{1,0:T(8,128)(2,1)}, u32[]{:S(2)}, u32[]{:S(2)}) collective-permute-start(bf16[2048,768]{1,0:T(8,128)(2,1)S(1)} %concatenate.62), channel_id=1, source_target_pairs={{0,4},{4,0},{8,12},{12,8},{16,20},{20,16},{24,28},{28,24},{32,36},... | collective-permute-start | bytes 9437192 | tf_op jit(solution)/shard_map/ppermute | solution.py:105
  210.7 8.4 %slice-start = ((s8[4456448]{0:T(1024)(128)(4,1)}), s8[4194304]{0:T(1024)(128)(4,1)S(1)}, s32[]{:S(2)}) async-start(s8[4456448]{0:T(1024)(128)(4,1)} %bitcast.101), calls=%async_computation.11 | async-start | bytes 8388608
  212.1 5.4 %copy-start.2 = (bf16[1,64,32,64]{3,2,1,0:T(8,128)(2,1)S(1)}, bf16[1,64,32,64]{3,2,1,0:T(8,128)(2,1)}, u32[]{:S(2)}) copy-start(bf16[1,64,32,64]{3,2,1,0:T(8,128)(2,1)} %get-tuple-element.36) | copy-start | bytes 786436
  212.1 5.4 %copy-start.3 = (bf16[1,64,32,64]{3,2,1,0:T(8,128)(2,1)S(1)}, bf16[1,64,32,64]{3,2,1,0:T(8,128)(2,1)}, u32[]{:S(2)}) copy-start(bf16[1,64,32,64]{3,2,1,0:T(8,128)(2,1)} %get-tuple-element.37) | copy-start | bytes 786436
  212.1 5.4 %copy-start.4 = (bf16[1,64,32,64]{3,2,1,0:T(8,128)(2,1)S(1)}, bf16[1,64,32,64]{3,2,1,0:T(8,128)(2,1)}, u32[]{:S(2)}) copy-start(bf16[1,64,32,64]{3,2,1,0:T(8,128)(2,1)} %get-tuple-element.38) | copy-start | bytes 786436
  212.1 5.4 %copy-start.5 = (bf16[1,64,32,64]{3,2,1,0:T(8,128)(2,1)S(1)}, bf16[1,64,32,64]{3,2,1,0:T(8,128)(2,1)}, u32[]{:S(2)}) copy-start(bf16[1,64,32,64]{3,2,1,0:T(8,128)(2,1)} %get-tuple-element.39) | copy-start | bytes 786436
  212.1 7.0 %slice-start.1 = ((s8[4456448]{0:T(1024)(128)(4,1)}), s8[262144]{0:T(1024)(128)(4,1)S(1)}, s32[]{:S(2)}) async-start(s8[4456448]{0:T(1024)(128)(4,1)} %bitcast.101), calls=%async_computation.12 | async-start | bytes 524288
  289.4 16.6 %all-to-all-start.4 = ((bf16[4,16,48,128]{3,2,1,0:T(8,128)(2,1)}), bf16[4,16,48,128]{3,2,1,0:T(8,128)(2,1)S(1)}, u32[]{:S(2)}, u32[]{:S(2)}) async-start(bf16[4,16,48,128]{3,2,1,0:T(8,128)(2,1)} %bitcast.22), calls=%async_computation.4 | async-start | bytes 1572864 | tf_op jit(solution)/shard_map/shared/all_to_all | solution.py:131
  305.9 9.3 %all-to-all-start.5 = ((bf16[4,32,512]{2,1,0:T(8,128)(2,1)}), bf16[4,32,512]{2,1,0:T(8,128)(2,1)S(1)}, u32[]{:S(2)}, u32[]{:S(2)}) async-start(bf16[4,32,512]{2,1,0:T(8,128)(2,1)} %fusion.43), calls=%async_computation.5 | async-start | bytes 262144 | tf_op jit(solution)/shard_map/shared/all_to_all | solution.py:133
  309.8 10.5 %copy-start.6 = (bf16[512,256]{1,0:T(8,128)(2,1)}, bf16[512,256]{1,0:T(8,128)(2,1)S(1)}, u32[]{:S(2)}) copy-start(bf16[512,256]{1,0:T(8,128)(2,1)S(1)} %pad_maximum_fusion.3) | copy-start | bytes 786436
  310.0 10.3 %copy-start.7 = (bf16[512,256]{1,0:T(8,128)(2,1)}, bf16[512,256]{1,0:T(8,128)(2,1)S(1)}, u32[]{:S(2)}) copy-start(bf16[512,256]{1,0:T(8,128)(2,1)S(1)} %pad_maximum_fusion.2) | copy-start | bytes 786436
  316.5 46.2 %all-to-all-start.6 = ((bf16[4,128,512]{2,1,0:T(8,128)(2,1)}), bf16[4,128,512]{2,1,0:T(8,128)(2,1)S(1)}, u32[]{:S(2)}, u32[]{:S(2)}) async-start(bf16[4,128,512]{2,1,0:T(8,128)(2,1)} %broadcast_in_dim.70), calls=%async_computation.6 | async-start | bytes 1048576 | tf_op jit(solution)/shard_map/shared/all_to_all | solution.py:14
  320.6 52.5 %copy-start.10 = (bf16[512,256]{1,0:T(8,128)(2,1)}, bf16[512,256]{1,0:T(8,128)(2,1)S(1)}, u32[]{:S(2)}) copy-start(bf16[512,256]{1,0:T(8,128)(2,1)S(1)} %pad_maximum_fusion.4) | copy-start | bytes 786436
  362.7 9.4 %all-to-all-start.7 = ((bf16[4,32,512]{2,1,0:T(8,128)(2,1)}), bf16[4,32,512]{2,1,0:T(8,128)(2,1)S(1)}, u32[]{:S(2)}, u32[]{:S(2)}) async-start(bf16[4,32,512]{2,1,0:T(8,128)(2,1)} %bitcast.59), calls=%async_computation.8 | async-start | bytes 262144 | tf_op jit(solution)/shard_map/all_to_all | solution.py:144
Sparse Core Ops, SparseCore 0:
  20.6 190.1 all-gather.2
  227.9 133.2 reduce-scatter.1

commit v3 on v2

--- a/solution.py
+++ b/solution.py
@@ -42,6 +42,28 @@
 def pack_down(down):
     half = down.shape[-2] // 2
     return jnp.concatenate([down[..., :half, :], down[..., half:, :]], axis=-1)
+
+
+def ring_sum(parts, n_fs, fs):
+    n = n_fs // 2
+    z = fs // 2
+    half = n // 2
+    ahead = [(i, (i + 2) % n_fs) for i in range(n_fs)]
+    behind = [(i, (i - 2) % n_fs) for i in range(n_fs)]
+
+    def part(k):
+        return lax.dynamic_index_in_dim(parts, (z + k) % n, 0, keepdims=False)
+
+    up, down = part(half), part(half + 1)
+    for k in range(half - 1, -1, -1):
+        up = lax.ppermute(up, "fs", ahead)
+        if k < half - 1:
+            down = lax.ppermute(down, "fs", behind)
+        if k:
+            up = up + part(k)
+            if k < half - 1:
+                down = down + part(n - k)
+    return (up.astype(F32) + down.astype(F32) + part(0).astype(F32)).astype(BF16)
 
 
 def on_device(
@@ -93,40 +115,25 @@
     n_grp = lax.axis_size("grp")
     cut = packed.shape[1] // n_grp
     piece = lax.dynamic_slice_in_dim(packed, lax.axis_index("grp") * cut, cut, 1)
-    payload, piece = lax.optimization_barrier((payload, piece))
+    shared_packed = pack(
+        (shared_gate * gain).astype(BF16),
+        (shared_up * gain).astype(BF16),
+        shared_down.astype(BF16),
+    )
+    payload, piece, shared_packed = lax.optimization_barrier((payload, piece, shared_packed))
     with jax.named_scope("tok_ag"):
         everyone = lax.all_gather(payload, "fs", axis=0, tiled=True, axis_index_groups=rings)
     with jax.named_scope("weights"):
         piece = lax.all_to_all(piece, "fs", 0, 0, tiled=True)
+        common = lax.all_gather(shared_packed, "fs", axis=0)
+        piece, common = lax.optimization_barrier((piece, common))
         pieces = broadcast_gather(piece, "grp")
         column = jnp.concatenate([pieces[i] for i in range(n_grp)], axis=1)
         gate, up, down = unpack(broadcast_gather(column, "tp"), local_rows)
     own = jnp.concatenate([gate, up, down], axis=1)
     other = lax.ppermute(own, "fs", swap)
 
-    rows = everyone[:, :width]
-    weights = everyone[:, width:].astype(F32)
-    lanes = jnp.arange(2 * experts, dtype=jnp.int32) % experts
-    partial = 0.0
-    for w, e in ((own, fs), (other, fs ^ 1)):
-        both = mm(rows, w[:, : 2 * hid]) * width**-0.5
-        share = jnp.sum(jnp.where(lanes == e, weights, 0.0), axis=1, keepdims=True)
-        hidden = (jax.nn.silu(both[:, :hid]) * both[:, hid:] * (share * hid**-0.5)).astype(BF16)
-        partial = partial + mm_t(hidden, w[:, 2 * hid :])
-    partial = partial.astype(BF16)
-
-    packed = pack(
-        (shared_gate * gain).astype(BF16),
-        (shared_up * gain).astype(BF16),
-        shared_down.astype(BF16),
-    )
-    partial, packed, normed = lax.optimization_barrier((partial, packed, normed))
-    with jax.named_scope("rs"):
-        routed = lax.psum_scatter(
-            partial, "fs", scatter_dimension=0, tiled=True, axis_index_groups=rings
-        )
     with jax.named_scope("shared"):
-        common = lax.all_gather(packed, "fs", axis=0)
         common = common.reshape(n_tp, n_fs // n_tp, *common.shape[1:])
         common = lax.all_to_all(common, "tp", 0, 0, tiled=True)
         common_gate, common_up, common_down = unpack(common, local_rows)
@@ -134,6 +141,35 @@
         part = jnp.concatenate([mm(back, common_gate), mm(back, common_up)], axis=1)
         part = (part * width**-0.5).astype(BF16)
         total = broadcast_gather(part, "tp").astype(F32).sum(axis=0)
+
+    everyone, total = lax.optimization_barrier((everyone, total))
+    rows = everyone[:, :width]
+    weights = everyone[:, width:].astype(F32)
+    lanes = jnp.arange(2 * experts, dtype=jnp.int32) % experts
+    hiddens = []
+    for w, e in ((own, fs), (other, fs ^ 1)):
+        both = mm(rows, w[:, : 2 * hid]) * width**-0.5
+        share = jnp.sum(jnp.where(lanes == e, weights, 0.0), axis=1, keepdims=True)
+        hiddens.append(
+            (jax.nn.silu(both[:, :hid]) * both[:, hid:] * (share * hid**-0.5)).astype(BF16)
+        )
+
+    def outputs(low, high):
+        return (
+            mm_t(hiddens[0], own[low:high, 2 * hid :]) + mm_t(hiddens[1], other[low:high, 2 * hid :])
+        ).astype(BF16)
+
+    edge = width * 5 // 8
+    first = outputs(0, edge)
+    with jax.named_scope("rs"):
+        routed = lax.psum_scatter(
+            first, "fs", scatter_dimension=0, tiled=True, axis_index_groups=rings
+        )
+    second = outputs(edge, width).reshape(n_fs // 2, sub, width - edge)
+    with jax.named_scope("ring"):
+        beside = ring_sum(second, n_fs, fs)
+    routed = jnp.concatenate([routed, beside], axis=1)
+    with jax.named_scope("shared_out"):
         shared_hidden = (
             jax.nn.silu(total[:, :shared_hid]) * total[:, shared_hid:]
         ).astype(BF16)

time: 382 us -> 499 us (1.31)
  starting transfers between devices: 21.1 us -> 183 us
  blocking collectives: 215 us -> 110 us
  waiting for transfers between devices: 80 us -> 108 us
  other arithmetic: 8.76 us -> 27 us
  matrix products: 16.7 us -> 22.2 us
    ppermute x0 -> x31, starting transfers between devices: none -> 109 us  [the longest x16 54.7 us: ring_sum(): up = lax.ppermute(up, 'fs', ahead)]
    all_to_all x1 -> x0, blocking collectives: 104 us -> none  [on_device(): piece = lax.all_to_all(piece, 'fs', 0, 0, tiled=True)]
    ppermute x0 -> x31, waiting for transfers between devices: none -> 47.9 us  [the longest x15 33.7 us: ring_sum(): down = lax.ppermute(down, 'fs', behind)]
    all_to_all x0 -> x1, starting transfers between devices: none -> 47.3 us  [on_device(): piece = lax.all_to_all(piece, 'fs', 0, 0, tiled=True)]
    all_to_all x1 -> x2, waiting for transfers between devices: 0.01 us -> 43.9 us  [broadcast_gather(): lax.all_to_all(jnp.broadcast_to(shard[None], (length, *shard.shape)), axi...]
    reduce_scatter x1, waiting for transfers between devices: 40.6 us -> 0.02 us  [on_device(): lax.psum_scatter(first, 'fs', scatter_dimension=0, tiled=True, axis_index...]
    all_to_all x2 -> x1, blocking collectives: 49.8 us -> 13.2 us  [broadcast_gather(): lax.all_to_all(jnp.broadcast_to(shard[None], (length, *shard.shape)), axi...]
    all_gather x1, blocking collectives: 61.6 us -> 97.3 us  [on_device(): common = lax.all_gather(shared_packed, 'fs', axis=0)]
  transfers between devices with their start and end apart: 8 -> 41, of which waited for: 6 -> 31; matrix products, arithmetic and copies ran while one was open for 10% -> 13% of each run, Pallas kernels for 0% -> 0%
where the time goes in v3:
time: 499 us; the launch traced here: 495 us
  starting transfers between devices  183 us (37%)
  blocking collectives  110 us (22%)
  waiting for transfers between devices  108 us (22%)
  local copies, waits for them, and re-layouts  28.7 us (6%)
  other arithmetic  27 us (5%)
  matrix products  22.2 us (4%)
  between operations  15.5 us (3%)
    all_gather x1, blocking collectives, on_device(): common = lax.all_gather(shared_packed, 'fs', axis=0)  97.3 us
    ppermute x16, starting transfers between devices, ring_sum(): up = lax.ppermute(up, 'fs', ahead)  54.7 us
    ppermute x15, starting transfers between devices, ring_sum(): down = lax.ppermute(down, 'fs', behind)  54.2 us
    all_to_all x1, starting transfers between devices, on_device(): piece = lax.all_to_all(piece, 'fs', 0, 0, tiled=True)  47.3 us
    all_to_all x2, waiting for transfers between devices, broadcast_gather(): lax.all_to_all(jnp.broadcast_to(shard[None], (length, *shard.shape)), axi...  43.9 us
    ppermute x15, waiting for transfers between devices, ring_sum(): down = lax.ppermute(down, 'fs', behind)  33.7 us
    ppermute x16, waiting for transfers between devices, ring_sum(): up = lax.ppermute(up, 'fs', ahead)  14.2 us
    concatenate x2, local copies, waits for them, and re-layouts, on_device(): own = jnp.concatenate([gate, up, down], axis=1)  13.4 us
  transfers between devices with their start and end apart: 41, of which 31 were waited for; matrix products, arithmetic and copies ran while one was open for 13% of the time, Pallas kernels for 0%

profile of v3, /device:TPU:40, one launch (start us, length us, event | category | flops | bytes accessed | tf_op | source)
XLA Modules:
  0.0 495.0 jit_solution(3017249803304096660)
XLA Ops:
  7.2 4.7 all-to-all-start
  20.5 47.3 %all-to-all-start.1 = ((bf16[64,24,128]{2,1,0:T(8,128)(2,1)}), bf16[64,24,128]{2,1,0:T(8,128)(2,1)S(1)}, u32[]{:S(2)}, u32[]{:S(2)}) async-start(bf16[64,24,128]{2,1,0:T(8,128)(2,1)} %fusion.28), calls=%async_computation.1 | async-start | bytes 786432 | tf_op jit(solution)/shard_map/weights/all_to_all | solution.py:127
  67.8 97.3 %all-gather = bf16[3072,128]{1,0:T(8,128)(2,1)} all-gather(bf16[48,128]{1,0:T(8,128)(2,1)S(1)} %maximum_maximum_fusion), channel_id=2, replica_groups=mesh['grp'=2,'fs'=64,'tp'=4] {'fs'}, dimensions={0}, use_global_device_ids=true | all-gather | bytes 798720 | tf_op jit(solution)/shard_map/weights/all_gather | solution.py:128
  165.2 13.2 %all_to_all.40 = bf16[2,64,24,128]{3,2,1,0:T(8,128)(2,1)S(1)} all-to-all(bf16[2,64,24,128]{3,2,1,0:T(8,128)(2,1)S(1)} %broadcast_in_dim.62), channel_id=1, replica_groups=mesh['grp'=2,'fs'=64,'tp'=4] {'grp'}, dimensions={0} | all-to-all | bytes 1572864 | tf_op jit(solution)/shard_map/weights/all_to_all | solution.py:14
  178.4 4.9 all-to-all-start.4
  183.5 11.8 %all-to-all-done.4 = bf16[4,16,48,128]{3,2,1,0:T(8,128)(2,1)S(1)} async-done(((bf16[4,16,48,128]{3,2,1,0:T(8,128)(2,1)}), bf16[4,16,48,128]{3,2,1,0:T(8,128)(2,1)S(1)}, u32[]{:S(2)}, u32[]{:S(2)}) %all-to-all-start.4) | async-done | bytes 786464 | tf_op jit(solution)/shard_map/shared/all_to_all | solution.py:138
  195.2 2.1 broadcast_in_dim.63
  197.3 3.8 all-to-all-start.3
  203.8 33.7 %all-to-all-done.3 = bf16[4,64,48,128]{3,2,1,0:T(8,128)(2,1)S(1)} async-done(((bf16[4,64,48,128]{3,2,1,0:T(8,128)(2,1)}), bf16[4,64,48,128]{3,2,1,0:T(8,128)(2,1)S(1)}, u32[]{:S(2)}, u32[]{:S(2)}) %all-to-all-start.3) | async-done | bytes 3145760 | tf_op jit(solution)/shard_map/weights/all_to_all | solution.py:14
  237.4 3.4 all-to-all-start.5
  241.3 2.6 fusion.52
  245.5 6.9 %concatenate.68 = bf16[2048,768]{1,0:T(8,128)(2,1)S(1)} concatenate(bf16[2048,64]{1,0:T(8,128)(2,1)} %bitcast.141, bf16[2048,64]{1,0:T(8,128)(2,1)} %bitcast.139, bf16[2048,64]{1,0:T(8,128)(2,1)} %bitcast.137, bf16[2048,64]{1,0:T(8,128)(2,1)} %bitcast.135, bf16[2048,64]{1,0:T(8,128)(2,1)} %bitcast.133, bf16[2048,64]{1,0:T(8,128)(2,1)} %bitcast.131, bf16[2048,64]{1,0:T(8,128)(2,1)} %bitcast.129, ...), dimensions={1} | concatenate | bytes 6291456 | tf_op jit(solution)/shard_map/concatenate | solution.py:133
  256.7 4.7 all-to-all-start.6
  261.4 10.2 %all-to-all-done.6 = bf16[4,128,512]{2,1,0:T(8,128)(2,1)} async-done(((bf16[4,128,512]{2,1,0:T(8,128)(2,1)}), bf16[4,128,512]{2,1,0:T(8,128)(2,1)}, u32[]{:S(2)}, u32[]{:S(2)}) %all-to-all-start.6) | async-done | bytes 524320 | tf_op jit(solution)/shard_map/shared/all_to_all | solution.py:14
  272.8 6.5 %concatenate.74 = bf16[2048,512]{1,0:T(8,128)(2,1)} concatenate(bf16[2048,64]{1,0:T(8,128)(2,1)} %bitcast.142, bf16[2048,64]{1,0:T(8,128)(2,1)} %bitcast.140, bf16[2048,64]{1,0:T(8,128)(2,1)} %bitcast.138, bf16[2048,64]{1,0:T(8,128)(2,1)} %bitcast.136, bf16[2048,64]{1,0:T(8,128)(2,1)} %bitcast.134, bf16[2048,64]{1,0:T(8,128)(2,1)} %bitcast.132, bf16[2048,64]{1,0:T(8,128)(2,1)} %bitcast.130, ...), dimensions={1} | concatenate | bytes 4194304 | tf_op jit(solution)/shard_map/concatenate | solution.py:133
  279.2 3.2 pad_maximum_fusion
  283.6 5.3 %fusion.5 = f32[1024,512]{1,0:T(8,128)S(1)} fusion(bf16[2048,512]{1,0:T(8,128)(2,1)} %concatenate.74, bf16[1024,2176]{1,0:T(8,128)(2,1)} %all-gather.3.cloned.1.call-done), kind=kOutput, calls=%fused_computation.13 | convolution fusion | flops 2148007936 | bytes 8388608 | tf_op jit(solution)/shard_map/dot_general | solution.py:20
  289.0 2.6 fusion.31
  293.9 3.9 fusion.8
  299.1 3.6 add_convert_fusion
  302.8 3.4 add_convert_fusion.1
  308.3 5.2 %collective-permute-start.17 = (bf16[32,768]{1,0:T(8,128)(2,1)S(1)}, bf16[32,768]{1,0:T(8,128)(2,1)S(1)}, u32[]{:S(2)}, u32[]{:S(2)}) collective-permute-start(bf16[32,768]{1,0:T(8,128)(2,1)S(1)} %get-tuple-element.73), channel_id=1, source_target_pairs={{0,248},{4,252},{8,0},{12,4},{16,8},{20,12},{24,16},{28,20},{32,24... | collective-permute-start | bytes 147464 | tf_op jit(solution)/shard_map/ring/ppermute | solution.py:61
  315.5 5.2 %collective-permute-done.2 = bf16[32,768]{1,0:T(8,128)(2,1)S(1)} collective-permute-done((bf16[32,768]{1,0:T(8,128)(2,1)S(1)}, bf16[32,768]{1,0:T(8,128)(2,1)S(1)}, u32[]{:S(2)}, u32[]{:S(2)}) %collective-permute-start.2) | collective-permute-done | bytes 49184 | tf_op jit(solution)/shard_map/ring/ppermute | solution.py:59
  320.8 2.1 collective-permute-start.3
  322.9 5.2 %collective-permute-start.18 = (bf16[32,768]{1,0:T(8,128)(2,1)S(1)}, bf16[32,768]{1,0:T(8,128)(2,1)S(1)}, u32[]{:S(2)}, u32[]{:S(2)}) collective-permute-start(bf16[32,768]{1,0:T(8,128)(2,1)S(1)} %get-tuple-element.71), channel_id=1, source_target_pairs={{0,248},{4,252},{8,0},{12,4},{16,8},{20,12},{24,16},{28,20},{32,24... | collective-permute-start | bytes 147464 | tf_op jit(solution)/shard_map/ring/ppermute | solution.py:61
  330.6 2.1 collective-permute-start.4
  332.8 5.3 %collective-permute-start.19 = (bf16[32,768]{1,0:T(8,128)(2,1)S(1)}, bf16[32,768]{1,0:T(8,128)(2,1)S(1)}, u32[]{:S(2)}, u32[]{:S(2)}) collective-permute-start(bf16[32,768]{1,0:T(8,128)(2,1)S(1)} %get-tuple-element.69), channel_id=1, source_target_pairs={{0,248},{4,252},{8,0},{12,4},{16,8},{20,12},{24,16},{28,20},{32,24... | collective-permute-start | bytes 147464 | tf_op jit(solution)/shard_map/ring/ppermute | solution.py:61
  338.2 2.0 collective-permute-done.19
  341.1 4.8 collective-permute-start.5
  345.9 2.8 collective-permute-start.20
  349.2 3.4 collective-permute-done.20
  353.4 3.4 collective-permute-start.6
  356.8 3.7 collective-permute-start.21
  360.9 2.1 collective-permute-done.21
  363.8 3.1 collective-permute-start.7
  366.9 4.0 collective-permute-start.22
  371.7 2.1 collective-permute-done.22
  374.7 3.9 collective-permute-start.8
  378.6 3.2 collective-permute-start.23
  382.4 2.8 collective-permute-done.23
  386.0 3.7 collective-permute-start.9
  389.7 3.4 collective-permute-start.24
  396.7 3.9 collective-permute-start.10
  400.6 3.2 collective-permute-start.25
  404.4 2.3 collective-permute-done.25
  407.6 5.4 %collective-permute-start.11 = (bf16[32,768]{1,0:T(8,128)(2,1)S(1)}, bf16[32,768]{1,0:T(8,128)(2,1)S(1)}, u32[]{:S(2)}, u32[]{:S(2)}) collective-permute-start(bf16[32,768]{1,0:T(8,128)(2,1)S(1)} %get-tuple-element.54), channel_id=1, source_target_pairs={{0,8},{4,12},{8,16},{12,20},{16,24},{20,28},{24,32},{28,36},{32,40... | collective-permute-start | bytes 147464 | tf_op jit(solution)/shard_map/ring/ppermute | solution.py:59
  415.1 4.3 collective-permute-done.26
  420.2 4.8 collective-permute-start.12
  425.0 2.3 collective-permute-start.27
  427.7 3.3 collective-permute-done.27
  431.8 3.9 collective-permute-start.13
  435.8 3.2 collective-permute-start.28
  439.1 2.7 collective-permute-done.28
  442.7 3.6 collective-permute-start.14
  446.2 3.5 collective-permute-start.29
  449.9 2.3 collective-permute-done.29
  453.1 4.1 collective-permute-start.15
  457.2 3.0 collective-permute-start.30
  460.3 2.9 collective-permute-done.30
  464.1 4.2 collective-permute-start.31
  470.5 5.0 %collective-permute-done.16 = bf16[32,768]{1,0:T(8,128)(2,1)S(1)} collective-permute-done((bf16[32,768]{1,0:T(8,128)(2,1)S(1)}, bf16[32,768]{1,0:T(8,128)(2,1)S(1)}, u32[]{:S(2)}, u32[]{:S(2)}) %collective-permute-start.16) | collective-permute-done | bytes 49184 | tf_op jit(solution)/shard_map/ring/ppermute | solution.py:59
  477.9 3.4 all-to-all-start.7
  481.4 2.0 dynamic-slice_bitcast_fusion
  483.4 3.9 all-to-all-done.7
  (133 shorter events, 53.5 us)
Async XLA Ops:
  7.2 6.4 %copy-start = (s32[128,8]{0,1:T(8,128)S(1)}, s32[128,8]{0,1:T(8,128)}, u32[]{:S(2)}) copy-start(s32[128,8]{0,1:T(8,128)} %param.11) | copy-start | bytes 12292
  7.2 8.1 %copy-start.17 = (f32[32,64]{1,0:T(8,128)S(1)}, f32[32,64]{1,0:T(8,128)}, u32[]{:S(2)}) copy-start(f32[32,64]{1,0:T(8,128)} %param.19) | copy-start | bytes 24580
  7.2 8.1 %copy-start.10 = (f32[64,32,64]{2,1,0:T(8,128)S(1)}, f32[64,32,64]{2,1,0:T(8,128)}, u32[]{:S(2)}) copy-start(f32[64,32,64]{2,1,0:T(8,128)} %param.15) | copy-start | bytes 1572868
  7.2 8.1 %copy-start.19 = (f32[32]{0:T(128)S(1)}, f32[32]{0:T(128)}, u32[]{:S(2)}) copy-start(f32[32]{0:T(128)} %param.13) | copy-start | bytes 388
  7.2 8.1 %copy-start.11 = (f32[64,32,64]{2,1,0:T(8,128)S(1)}, f32[64,32,64]{2,1,0:T(8,128)}, u32[]{:S(2)}) copy-start(f32[64,32,64]{2,1,0:T(8,128)} %param.14) | copy-start | bytes 1572868
  7.2 10.7 %all-to-all-start = ((bf16[4,32,512]{2,1,0:T(8,128)(2,1)}), bf16[4,32,512]{2,1,0:T(8,128)(2,1)S(1)}, u32[]{:S(2)}, u32[]{:S(2)}) async-start(bf16[4,32,512]{2,1,0:T(8,128)(2,1)} %bitcast.187), calls=%async_computation | async-start | bytes 262144 | tf_op jit(solution)/shard_map/all_to_all | solution.py:93
  12.0 270.4 %all-gather.3.cloned.1.call-start = ((), (), s32[]{:S(2)}) async-start(), calls=%async_computation.9 | async-start | bytes 4595712 | tf_op jit(solution)/shard_map/tok_ag/all_gather | solution.py:125
  15.2 0.7 copy-start.15
  15.2 0.7 copy-start.16
  20.5 144.6 %all-to-all-start.1 = ((bf16[64,24,128]{2,1,0:T(8,128)(2,1)}), bf16[64,24,128]{2,1,0:T(8,128)(2,1)S(1)}, u32[]{:S(2)}, u32[]{:S(2)}) async-start(bf16[64,24,128]{2,1,0:T(8,128)(2,1)} %fusion.28), calls=%async_computation.1 | async-start | bytes 786432 | tf_op jit(solution)/shard_map/weights/all_to_all | solution.py:127
  178.4 16.9 %all-to-all-start.4 = ((bf16[4,16,48,128]{3,2,1,0:T(8,128)(2,1)}), bf16[4,16,48,128]{3,2,1,0:T(8,128)(2,1)S(1)}, u32[]{:S(2)}, u32[]{:S(2)}) async-start(bf16[4,16,48,128]{3,2,1,0:T(8,128)(2,1)} %bitcast.23), calls=%async_computation.4 | async-start | bytes 1572864 | tf_op jit(solution)/shard_map/shared/all_to_all | solution.py:138
  195.2 2.1 copy-start.1
  197.3 40.1 %all-to-all-start.3 = ((bf16[4,64,48,128]{3,2,1,0:T(8,128)(2,1)}), bf16[4,64,48,128]{3,2,1,0:T(8,128)(2,1)S(1)}, u32[]{:S(2)}, u32[]{:S(2)}) async-start(bf16[4,64,48,128]{3,2,1,0:T(8,128)(2,1)} %broadcast_in_dim.63), calls=%async_computation.3 | async-start | bytes 6291456 | tf_op jit(solution)/shard_map/weights/all_to_all | solution.py:14
  203.7 51.8 %copy-start.12 = (bf16[512,256]{1,0:T(8,128)(2,1)}, bf16[512,256]{1,0:T(8,128)(2,1)S(1)}, u32[]{:S(2)}) copy-start(bf16[512,256]{1,0:T(8,128)(2,1)S(1)} %get-tuple-element.106) | copy-start | bytes 786436
  237.4 17.0 %all-to-all-start.5 = ((bf16[4,32,512]{2,1,0:T(8,128)(2,1)}), bf16[4,32,512]{2,1,0:T(8,128)(2,1)S(1)}, u32[]{:S(2)}, u32[]{:S(2)}) async-start(bf16[4,32,512]{2,1,0:T(8,128)(2,1)} %fusion.40), calls=%async_computation.5 | async-start | bytes 262144 | tf_op jit(solution)/shard_map/shared/all_to_all | solution.py:140
  252.4 30.0 %copy-start.3 = (bf16[2048,768]{1,0:T(8,128)(2,1)}, bf16[2048,768]{1,0:T(8,128)(2,1)S(1)}, u32[]{:S(2)}) copy-start(bf16[2048,768]{1,0:T(8,128)(2,1)S(1)} %concatenate.68) | copy-start | bytes 9437188
  252.4 40.2 %collective-permute-start = (bf16[2048,768]{1,0:T(8,128)(2,1)S(1)}, bf16[2048,768]{1,0:T(8,128)(2,1)}, u32[]{:S(2)}, u32[]{:S(2)}) collective-permute-start(bf16[2048,768]{1,0:T(8,128)(2,1)S(1)} %concatenate.68), channel_id=1, source_target_pairs={{0,4},{4,0},{8,12},{12,8},{16,20},{20,16},{24,28},{28,24},{32,36},... | collective-permute-start | bytes 9437192 | tf_op jit(solution)/shard_map/ppermute | solution.py:134
  256.7 15.0 %all-to-all-start.6 = ((bf16[4,128,512]{2,1,0:T(8,128)(2,1)}), bf16[4,128,512]{2,1,0:T(8,128)(2,1)}, u32[]{:S(2)}, u32[]{:S(2)}) async-start(bf16[4,128,512]{2,1,0:T(8,128)(2,1)} %broadcast_in_dim.67), calls=%async_computation.6 | async-start | bytes 1048576 | tf_op jit(solution)/shard_map/shared/all_to_all | solution.py:14
  261.4 215.0 %reduce-scatter.2.cloned.1.call-start = ((), (), s32[]{:S(2)}) async-start(), calls=%async_computation.10 | async-start | bytes 2703360 | tf_op jit(solution)/shard_map/rs/reduce_scatter | solution.py:165
  283.6 5.4 %copy-start.4 = (bf16[1,64,32,64]{3,2,1,0:T(8,128)(2,1)S(1)}, bf16[1,64,32,64]{3,2,1,0:T(8,128)(2,1)}, u32[]{:S(2)}) copy-start(bf16[1,64,32,64]{3,2,1,0:T(8,128)(2,1)} %get-tuple-element.40) | copy-start | bytes 786436
  283.6 5.4 %copy-start.5 = (bf16[1,64,32,64]{3,2,1,0:T(8,128)(2,1)S(1)}, bf16[1,64,32,64]{3,2,1,0:T(8,128)(2,1)}, u32[]{:S(2)}) copy-start(bf16[1,64,32,64]{3,2,1,0:T(8,128)(2,1)} %get-tuple-element.41) | copy-start | bytes 786436
  283.6 5.4 %copy-start.6 = (bf16[1,64,32,64]{3,2,1,0:T(8,128)(2,1)S(1)}, bf16[1,64,32,64]{3,2,1,0:T(8,128)(2,1)}, u32[]{:S(2)}) copy-start(bf16[1,64,32,64]{3,2,1,0:T(8,128)(2,1)} %get-tuple-element.42) | copy-start | bytes 786436
  283.6 5.4 %copy-start.7 = (bf16[1,64,32,64]{3,2,1,0:T(8,128)(2,1)S(1)}, bf16[1,64,32,64]{3,2,1,0:T(8,128)(2,1)}, u32[]{:S(2)}) copy-start(bf16[1,64,32,64]{3,2,1,0:T(8,128)(2,1)} %get-tuple-element.43) | copy-start | bytes 786436
  289.0 2.6 copy-start.9
  291.6 2.3 copy-start.18
  297.8 1.3 copy-start.13
  306.3 23.5 %copy-start.8 = (bf16[1024,768]{1,0:T(8,128)(2,1)}, bf16[1024,768]{1,0:T(8,128)(2,1)S(1)}, u32[]{:S(2)}) copy-start(bf16[1024,768]{1,0:T(8,128)(2,1)S(1)} %add_convert_fusion.1) | copy-start | bytes 4718596
  306.3 7.2 %collective-permute-start.1 = (bf16[32,768]{1,0:T(8,128)(2,1)S(1)}, bf16[32,768]{1,0:T(8,128)(2,1)S(1)}, u32[]{:S(2)}, u32[]{:S(2)}) collective-permute-start(bf16[32,768]{1,0:T(8,128)(2,1)S(1)} %get-tuple-element.72), channel_id=1, source_target_pairs={{0,8},{4,12},{8,16},{12,20},{16,24},{20,28},{24,32},{28,36},{32,40... | collective-permute-start | bytes 147464 | tf_op jit(solution)/shard_map/ring/ppermute | solution.py:59
  308.3 7.3 %collective-permute-start.17 = (bf16[32,768]{1,0:T(8,128)(2,1)S(1)}, bf16[32,768]{1,0:T(8,128)(2,1)S(1)}, u32[]{:S(2)}, u32[]{:S(2)}) collective-permute-start(bf16[32,768]{1,0:T(8,128)(2,1)S(1)} %get-tuple-element.73), channel_id=1, source_target_pairs={{0,248},{4,252},{8,0},{12,4},{16,8},{20,12},{24,16},{28,20},{32,24... | collective-permute-start | bytes 147464 | tf_op jit(solution)/shard_map/ring/ppermute | solution.py:61
  313.5 7.2 %collective-permute-start.2 = (bf16[32,768]{1,0:T(8,128)(2,1)S(1)}, bf16[32,768]{1,0:T(8,128)(2,1)S(1)}, u32[]{:S(2)}, u32[]{:S(2)}) collective-permute-start(bf16[32,768]{1,0:T(8,128)(2,1)S(1)} %bitcast_add_fusion.28), channel_id=1, source_target_pairs={{0,8},{4,12},{8,16},{12,20},{16,24},{20,28},{24,32},{28,36},{32,40... | collective-permute-start | bytes 147464 | tf_op jit(solution)/shard_map/ring/ppermute | solution.py:59
  320.8 129.0 %copy-start.2 = (bf16[4,16,48,128]{3,2,1,0:T(8,128)(2,1)S(1)}, bf16[4,16,48,128]{3,2,1,0:T(8,128)(2,1)}, u32[]{:S(2)}) copy-start(bf16[4,16,48,128]{3,2,1,0:T(8,128)(2,1)} %copy-done.1) | copy-start | bytes 2359300
  320.8 7.4 %collective-permute-start.3 = (bf16[32,768]{1,0:T(8,128)(2,1)S(1)}, bf16[32,768]{1,0:T(8,128)(2,1)S(1)}, u32[]{:S(2)}, u32[]{:S(2)}) collective-permute-start(bf16[32,768]{1,0:T(8,128)(2,1)S(1)} %get-tuple-element.70), channel_id=1, source_target_pairs={{0,8},{4,12},{8,16},{12,20},{16,24},{20,28},{24,32},{28,36},{32,40... | collective-permute-start | bytes 147464 | tf_op jit(solution)/shard_map/ring/ppermute | solution.py:59
  322.9 6.9 %collective-permute-start.18 = (bf16[32,768]{1,0:T(8,128)(2,1)S(1)}, bf16[32,768]{1,0:T(8,128)(2,1)S(1)}, u32[]{:S(2)}, u32[]{:S(2)}) collective-permute-start(bf16[32,768]{1,0:T(8,128)(2,1)S(1)} %get-tuple-element.71), channel_id=1, source_target_pairs={{0,248},{4,252},{8,0},{12,4},{16,8},{20,12},{24,16},{28,20},{32,24... | collective-permute-start | bytes 147464 | tf_op jit(solution)/shard_map/ring/ppermute | solution.py:61
  330.6 7.6 %collective-permute-start.4 = (bf16[32,768]{1,0:T(8,128)(2,1)S(1)}, bf16[32,768]{1,0:T(8,128)(2,1)S(1)}, u32[]{:S(2)}, u32[]{:S(2)}) collective-permute-start(bf16[32,768]{1,0:T(8,128)(2,1)S(1)} %get-tuple-element.68), channel_id=1, source_target_pairs={{0,8},{4,12},{8,16},{12,20},{16,24},{20,28},{24,32},{28,36},{32,40... | collective-permute-start | bytes 147464 | tf_op jit(solution)/shard_map/ring/ppermute | solution.py:59
  332.8 7.5 %collective-permute-start.19 = (bf16[32,768]{1,0:T(8,128)(2,1)S(1)}, bf16[32,768]{1,0:T(8,128)(2,1)S(1)}, u32[]{:S(2)}, u32[]{:S(2)}) collective-permute-start(bf16[32,768]{1,0:T(8,128)(2,1)S(1)} %get-tuple-element.69), channel_id=1, source_target_pairs={{0,248},{4,252},{8,0},{12,4},{16,8},{20,12},{24,16},{28,20},{32,24... | collective-permute-start | bytes 147464 | tf_op jit(solution)/shard_map/ring/ppermute | solution.py:61
  341.1 8.1 %collective-permute-start.5 = (bf16[32,768]{1,0:T(8,128)(2,1)S(1)}, bf16[32,768]{1,0:T(8,128)(2,1)S(1)}, u32[]{:S(2)}, u32[]{:S(2)}) collective-permute-start(bf16[32,768]{1,0:T(8,128)(2,1)S(1)} %get-tuple-element.66), channel_id=1, source_target_pairs={{0,8},{4,12},{8,16},{12,20},{16,24},{20,28},{24,32},{28,36},{32,40... | collective-permute-start | bytes 147464 | tf_op jit(solution)/shard_map/ring/ppermute | solution.py:59
  345.9 6.7 %collective-permute-start.20 = (bf16[32,768]{1,0:T(8,128)(2,1)S(1)}, bf16[32,768]{1,0:T(8,128)(2,1)S(1)}, u32[]{:S(2)}, u32[]{:S(2)}) collective-permute-start(bf16[32,768]{1,0:T(8,128)(2,1)S(1)} %get-tuple-element.67), channel_id=1, source_target_pairs={{0,248},{4,252},{8,0},{12,4},{16,8},{20,12},{24,16},{28,20},{32,24... | collective-permute-start | bytes 147464 | tf_op jit(solution)/shard_map/ring/ppermute | solution.py:61
  353.4 7.4 %collective-permute-start.6 = (bf16[32,768]{1,0:T(8,128)(2,1)S(1)}, bf16[32,768]{1,0:T(8,128)(2,1)S(1)}, u32[]{:S(2)}, u32[]{:S(2)}) collective-permute-start(bf16[32,768]{1,0:T(8,128)(2,1)S(1)} %get-tuple-element.64), channel_id=1, source_target_pairs={{0,8},{4,12},{8,16},{12,20},{16,24},{20,28},{24,32},{28,36},{32,40... | collective-permute-start | bytes 147464 | tf_op jit(solution)/shard_map/ring/ppermute | solution.py:59
  356.8 6.1 %collective-permute-start.21 = (bf16[32,768]{1,0:T(8,128)(2,1)S(1)}, bf16[32,768]{1,0:T(8,128)(2,1)S(1)}, u32[]{:S(2)}, u32[]{:S(2)}) collective-permute-start(bf16[32,768]{1,0:T(8,128)(2,1)S(1)} %get-tuple-element.65), channel_id=1, source_target_pairs={{0,248},{4,252},{8,0},{12,4},{16,8},{20,12},{24,16},{28,20},{32,24... | collective-permute-start | bytes 147464 | tf_op jit(solution)/shard_map/ring/ppermute | solution.py:61
  363.8 7.9 %collective-permute-start.7 = (bf16[32,768]{1,0:T(8,128)(2,1)S(1)}, bf16[32,768]{1,0:T(8,128)(2,1)S(1)}, u32[]{:S(2)}, u32[]{:S(2)}) collective-permute-start(bf16[32,768]{1,0:T(8,128)(2,1)S(1)} %get-tuple-element.62), channel_id=1, source_target_pairs={{0,8},{4,12},{8,16},{12,20},{16,24},{20,28},{24,32},{28,36},{32,40... | collective-permute-start | bytes 147464 | tf_op jit(solution)/shard_map/ring/ppermute | solution.py:59
  366.9 7.0 %collective-permute-start.22 = (bf16[32,768]{1,0:T(8,128)(2,1)S(1)}, bf16[32,768]{1,0:T(8,128)(2,1)S(1)}, u32[]{:S(2)}, u32[]{:S(2)}) collective-permute-start(bf16[32,768]{1,0:T(8,128)(2,1)S(1)} %get-tuple-element.63), channel_id=1, source_target_pairs={{0,248},{4,252},{8,0},{12,4},{16,8},{20,12},{24,16},{28,20},{32,24... | collective-permute-start | bytes 147464 | tf_op jit(solution)/shard_map/ring/ppermute | solution.py:61
  374.7 7.7 %collective-permute-start.8 = (bf16[32,768]{1,0:T(8,128)(2,1)S(1)}, bf16[32,768]{1,0:T(8,128)(2,1)S(1)}, u32[]{:S(2)}, u32[]{:S(2)}) collective-permute-start(bf16[32,768]{1,0:T(8,128)(2,1)S(1)} %get-tuple-element.60), channel_id=1, source_target_pairs={{0,8},{4,12},{8,16},{12,20},{16,24},{20,28},{24,32},{28,36},{32,40... | collective-permute-start | bytes 147464 | tf_op jit(solution)/shard_map/ring/ppermute | solution.py:59
  378.6 6.6 %collective-permute-start.23 = (bf16[32,768]{1,0:T(8,128)(2,1)S(1)}, bf16[32,768]{1,0:T(8,128)(2,1)S(1)}, u32[]{:S(2)}, u32[]{:S(2)}) collective-permute-start(bf16[32,768]{1,0:T(8,128)(2,1)S(1)} %get-tuple-element.61), channel_id=1, source_target_pairs={{0,248},{4,252},{8,0},{12,4},{16,8},{20,12},{24,16},{28,20},{32,24... | collective-permute-start | bytes 147464 | tf_op jit(solution)/shard_map/ring/ppermute | solution.py:61
  386.0 7.9 %collective-permute-start.9 = (bf16[32,768]{1,0:T(8,128)(2,1)S(1)}, bf16[32,768]{1,0:T(8,128)(2,1)S(1)}, u32[]{:S(2)}, u32[]{:S(2)}) collective-permute-start(bf16[32,768]{1,0:T(8,128)(2,1)S(1)} %get-tuple-element.58), channel_id=1, source_target_pairs={{0,8},{4,12},{8,16},{12,20},{16,24},{20,28},{24,32},{28,36},{32,40... | collective-permute-start | bytes 147464 | tf_op jit(solution)/shard_map/ring/ppermute | solution.py:59
  389.7 6.1 %collective-permute-start.24 = (bf16[32,768]{1,0:T(8,128)(2,1)S(1)}, bf16[32,768]{1,0:T(8,128)(2,1)S(1)}, u32[]{:S(2)}, u32[]{:S(2)}) collective-permute-start(bf16[32,768]{1,0:T(8,128)(2,1)S(1)} %get-tuple-element.59), channel_id=1, source_target_pairs={{0,248},{4,252},{8,0},{12,4},{16,8},{20,12},{24,16},{28,20},{32,24... | collective-permute-start | bytes 147464 | tf_op jit(solution)/shard_map/ring/ppermute | solution.py:61
  396.7 7.7 %collective-permute-start.10 = (bf16[32,768]{1,0:T(8,128)(2,1)S(1)}, bf16[32,768]{1,0:T(8,128)(2,1)S(1)}, u32[]{:S(2)}, u32[]{:S(2)}) collective-permute-start(bf16[32,768]{1,0:T(8,128)(2,1)S(1)} %get-tuple-element.56), channel_id=1, source_target_pairs={{0,8},{4,12},{8,16},{12,20},{16,24},{20,28},{24,32},{28,36},{32,40... | collective-permute-start | bytes 147464 | tf_op jit(solution)/shard_map/ring/ppermute | solution.py:59
  400.6 6.1 %collective-permute-start.25 = (bf16[32,768]{1,0:T(8,128)(2,1)S(1)}, bf16[32,768]{1,0:T(8,128)(2,1)S(1)}, u32[]{:S(2)}, u32[]{:S(2)}) collective-permute-start(bf16[32,768]{1,0:T(8,128)(2,1)S(1)} %get-tuple-element.57), channel_id=1, source_target_pairs={{0,248},{4,252},{8,0},{12,4},{16,8},{20,12},{24,16},{28,20},{32,24... | collective-permute-start | bytes 147464 | tf_op jit(solution)/shard_map/ring/ppermute | solution.py:61
  407.6 7.5 %collective-permute-start.11 = (bf16[32,768]{1,0:T(8,128)(2,1)S(1)}, bf16[32,768]{1,0:T(8,128)(2,1)S(1)}, u32[]{:S(2)}, u32[]{:S(2)}) collective-permute-start(bf16[32,768]{1,0:T(8,128)(2,1)S(1)} %get-tuple-element.54), channel_id=1, source_target_pairs={{0,8},{4,12},{8,16},{12,20},{16,24},{20,28},{24,32},{28,36},{32,40... | collective-permute-start | bytes 147464 | tf_op jit(solution)/shard_map/ring/ppermute | solution.py:59
  413.0 6.4 %collective-permute-start.26 = (bf16[32,768]{1,0:T(8,128)(2,1)S(1)}, bf16[32,768]{1,0:T(8,128)(2,1)S(1)}, u32[]{:S(2)}, u32[]{:S(2)}) collective-permute-start(bf16[32,768]{1,0:T(8,128)(2,1)S(1)} %get-tuple-element.55), channel_id=1, source_target_pairs={{0,248},{4,252},{8,0},{12,4},{16,8},{20,12},{24,16},{28,20},{32,24... | collective-permute-start | bytes 147464 | tf_op jit(solution)/shard_map/ring/ppermute | solution.py:61
  420.2 7.6 %collective-permute-start.12 = (bf16[32,768]{1,0:T(8,128)(2,1)S(1)}, bf16[32,768]{1,0:T(8,128)(2,1)S(1)}, u32[]{:S(2)}, u32[]{:S(2)}) collective-permute-start(bf16[32,768]{1,0:T(8,128)(2,1)S(1)} %get-tuple-element.52), channel_id=1, source_target_pairs={{0,8},{4,12},{8,16},{12,20},{16,24},{20,28},{24,32},{28,36},{32,40... | collective-permute-start | bytes 147464 | tf_op jit(solution)/shard_map/ring/ppermute | solution.py:59
  425.0 6.0 %collective-permute-start.27 = (bf16[32,768]{1,0:T(8,128)(2,1)S(1)}, bf16[32,768]{1,0:T(8,128)(2,1)S(1)}, u32[]{:S(2)}, u32[]{:S(2)}) collective-permute-start(bf16[32,768]{1,0:T(8,128)(2,1)S(1)} %get-tuple-element.53), channel_id=1, source_target_pairs={{0,248},{4,252},{8,0},{12,4},{16,8},{20,12},{24,16},{28,20},{32,24... | collective-permute-start | bytes 147464 | tf_op jit(solution)/shard_map/ring/ppermute | solution.py:61
  431.8 7.3 %collective-permute-start.13 = (bf16[32,768]{1,0:T(8,128)(2,1)S(1)}, bf16[32,768]{1,0:T(8,128)(2,1)S(1)}, u32[]{:S(2)}, u32[]{:S(2)}) collective-permute-start(bf16[32,768]{1,0:T(8,128)(2,1)S(1)} %get-tuple-element.50), channel_id=1, source_target_pairs={{0,8},{4,12},{8,16},{12,20},{16,24},{20,28},{24,32},{28,36},{32,40... | collective-permute-start | bytes 147464 | tf_op jit(solution)/shard_map/ring/ppermute | solution.py:59
  435.8 6.0 %collective-permute-start.28 = (bf16[32,768]{1,0:T(8,128)(2,1)S(1)}, bf16[32,768]{1,0:T(8,128)(2,1)S(1)}, u32[]{:S(2)}, u32[]{:S(2)}) collective-permute-start(bf16[32,768]{1,0:T(8,128)(2,1)S(1)} %get-tuple-element.51), channel_id=1, source_target_pairs={{0,248},{4,252},{8,0},{12,4},{16,8},{20,12},{24,16},{28,20},{32,24... | collective-permute-start | bytes 147464 | tf_op jit(solution)/shard_map/ring/ppermute | solution.py:61
  442.7 7.3 %collective-permute-start.14 = (bf16[32,768]{1,0:T(8,128)(2,1)S(1)}, bf16[32,768]{1,0:T(8,128)(2,1)S(1)}, u32[]{:S(2)}, u32[]{:S(2)}) collective-permute-start(bf16[32,768]{1,0:T(8,128)(2,1)S(1)} %get-tuple-element.48), channel_id=1, source_target_pairs={{0,8},{4,12},{8,16},{12,20},{16,24},{20,28},{24,32},{28,36},{32,40... | collective-permute-start | bytes 147464 | tf_op jit(solution)/shard_map/ring/ppermute | solution.py:59
  446.2 6.0 %collective-permute-start.29 = (bf16[32,768]{1,0:T(8,128)(2,1)S(1)}, bf16[32,768]{1,0:T(8,128)(2,1)S(1)}, u32[]{:S(2)}, u32[]{:S(2)}) collective-permute-start(bf16[32,768]{1,0:T(8,128)(2,1)S(1)} %get-tuple-element.49), channel_id=1, source_target_pairs={{0,248},{4,252},{8,0},{12,4},{16,8},{20,12},{24,16},{28,20},{32,24... | collective-permute-start | bytes 147464 | tf_op jit(solution)/shard_map/ring/ppermute | solution.py:61
  453.1 7.2 %collective-permute-start.15 = (bf16[32,768]{1,0:T(8,128)(2,1)S(1)}, bf16[32,768]{1,0:T(8,128)(2,1)S(1)}, u32[]{:S(2)}, u32[]{:S(2)}) collective-permute-start(bf16[32,768]{1,0:T(8,128)(2,1)S(1)} %get-tuple-element.46), channel_id=1, source_target_pairs={{0,8},{4,12},{8,16},{12,20},{16,24},{20,28},{24,32},{28,36},{32,40... | collective-permute-start | bytes 147464 | tf_op jit(solution)/shard_map/ring/ppermute | solution.py:59
  457.2 6.0 %collective-permute-start.30 = (bf16[32,768]{1,0:T(8,128)(2,1)S(1)}, bf16[32,768]{1,0:T(8,128)(2,1)S(1)}, u32[]{:S(2)}, u32[]{:S(2)}) collective-permute-start(bf16[32,768]{1,0:T(8,128)(2,1)S(1)} %get-tuple-element.47), channel_id=1, source_target_pairs={{0,248},{4,252},{8,0},{12,4},{16,8},{20,12},{24,16},{28,20},{32,24... | collective-permute-start | bytes 147464 | tf_op jit(solution)/shard_map/ring/ppermute | solution.py:61
  464.1 6.4 %collective-permute-start.31 = (bf16[32,768]{1,0:T(8,128)(2,1)S(1)}, bf16[32,768]{1,0:T(8,128)(2,1)S(1)}, u32[]{:S(2)}, u32[]{:S(2)}) collective-permute-start(bf16[32,768]{1,0:T(8,128)(2,1)S(1)} %get-tuple-element.45), channel_id=1, source_target_pairs={{0,248},{4,252},{8,0},{12,4},{16,8},{20,12},{24,16},{28,20},{32,24... | collective-permute-start | bytes 147464 | tf_op jit(solution)/shard_map/ring/ppermute | solution.py:61
  468.3 7.2 %collective-permute-start.16 = (bf16[32,768]{1,0:T(8,128)(2,1)S(1)}, bf16[32,768]{1,0:T(8,128)(2,1)S(1)}, u32[]{:S(2)}, u32[]{:S(2)}) collective-permute-start(bf16[32,768]{1,0:T(8,128)(2,1)S(1)} %get-tuple-element.44), channel_id=1, source_target_pairs={{0,8},{4,12},{8,16},{12,20},{16,24},{20,28},{24,32},{28,36},{32,40... | collective-permute-start | bytes 147464 | tf_op jit(solution)/shard_map/ring/ppermute | solution.py:59
  470.4 17.7 %copy-start.14 = (bf16[512,256]{1,0:T(8,128)(2,1)}, bf16[512,256]{1,0:T(8,128)(2,1)S(1)}, u32[]{:S(2)}) copy-start(bf16[512,256]{1,0:T(8,128)(2,1)S(1)} %pad_maximum_fusion.5) | copy-start | bytes 786436
  477.9 9.3 %all-to-all-start.7 = ((bf16[4,32,512]{2,1,0:T(8,128)(2,1)}), bf16[4,32,512]{2,1,0:T(8,128)(2,1)S(1)}, u32[]{:S(2)}, u32[]{:S(2)}) async-start(bf16[4,32,512]{2,1,0:T(8,128)(2,1)} %bitcast.126), calls=%async_computation.8 | async-start | bytes 262144 | tf_op jit(solution)/shard_map/all_to_all | solution.py:180
Sparse Core Ops, SparseCore 0:
  20.6 191.8 all-gather.2
  303.0 136.3 reduce-scatter.1

commit v4 on v2

--- a/solution.py
+++ b/solution.py
@@ -104,15 +104,19 @@
     own = jnp.concatenate([gate, up, down], axis=1)
     other = lax.ppermute(own, "fs", swap)
 
+    inward = jnp.concatenate([own[:, : 2 * hid], other[:, : 2 * hid]], axis=1)
+    outward = jnp.concatenate([own[:, 2 * hid :], other[:, 2 * hid :]], axis=1)
+    everyone, inward, outward = lax.optimization_barrier((everyone, inward, outward))
     rows = everyone[:, :width]
     weights = everyone[:, width:].astype(F32)
     lanes = jnp.arange(2 * experts, dtype=jnp.int32) % experts
-    partial = 0.0
-    for w, e in ((own, fs), (other, fs ^ 1)):
-        both = mm(rows, w[:, : 2 * hid]) * width**-0.5
+    both = mm(rows, inward) * width**-0.5
+    hiddens = []
+    for i, e in enumerate((fs, fs ^ 1)):
+        gated, raised = (both[:, k * hid : (k + 1) * hid] for k in (2 * i, 2 * i + 1))
         share = jnp.sum(jnp.where(lanes == e, weights, 0.0), axis=1, keepdims=True)
-        hidden = (jax.nn.silu(both[:, :hid]) * both[:, hid:] * (share * hid**-0.5)).astype(BF16)
-        partial = partial + mm_t(hidden, w[:, 2 * hid :])
+        hiddens.append((jax.nn.silu(gated) * raised * (share * hid**-0.5)).astype(BF16))
+    partial = mm_t(jnp.concatenate(hiddens, axis=1), outward)
     partial = partial.astype(BF16)
 
     packed = pack(

time: 382 us -> 386 us (1.010)
  blocking collectives: 215 us -> 115 us
  starting transfers between devices: 21.1 us -> 69.8 us
  waiting for transfers between devices: 80 us -> 125 us
  local copies, waits for them, and re-layouts: 23.9 us -> 35.1 us
    all_to_all x1 -> x0, blocking collectives: 104 us -> none  [on_device(): piece = lax.all_to_all(piece, 'fs', 0, 0, tiled=True)]
    all_to_all x0 -> x1, waiting for transfers between devices: none -> 51.7 us  [on_device(): piece = lax.all_to_all(piece, 'fs', 0, 0, tiled=True)]
    all_to_all x0 -> x1, starting transfers between devices: none -> 47.3 us  [on_device(): piece = lax.all_to_all(piece, 'fs', 0, 0, tiled=True)]
    concatenate x0 -> x2, local copies, waits for them, and re-layouts: none -> 13.6 us  [the longest x1 8.1 us: on_device(): inward = jnp.concatenate([own[:, :2 * hid], other[:, :2 * hid]], axis=1)]
    all_gather x1, waiting for transfers between devices: 15.7 us -> 4.29 us  [on_device(): lax.all_gather(payload, 'fs', axis=0, tiled=True, axis_index_groups=rings)]
    concatenate x2 -> x1, local copies, waits for them, and re-layouts: 13.5 us -> 6.98 us  [on_device(): own = jnp.concatenate([gate, up, down], axis=1)]
    ppermute x1, waiting for transfers between devices: 0.01 us -> 5.33 us  [on_device(): other = lax.ppermute(own, 'fs', swap)]
    slice x0 -> x2, local copies, waits for them, and re-layouts: none -> 4.19 us  [the longest x1 2.36 us: on_device(): outward = jnp.concatenate([own[:, 2 * hid:], other[:, 2 * hid:]], axis=1)]
  transfers between devices with their start and end apart: 8 -> 9, of which waited for: 6 -> 8; matrix products, arithmetic and copies ran while one was open for 10% -> 11% of each run, Pallas kernels for 0% -> 0%
where the time goes in v4:
time: 386 us; the launch traced here: 383 us
  waiting for transfers between devices  125 us (32%)
  blocking collectives  115 us (30%)
  starting transfers between devices  69.8 us (18%)
  local copies, waits for them, and re-layouts  35.1 us (9%)
  between operations  14.5 us (4%)
  matrix products  13.2 us (3%)
  other arithmetic  10.9 us (3%)
    all_gather x1, blocking collectives, on_device(): common = lax.all_gather(packed, 'fs', axis=0)  62.7 us
    all_to_all x2, blocking collectives, broadcast_gather(): lax.all_to_all(jnp.broadcast_to(shard[None], (length, *shard.shape)), axi...  52.2 us
    all_to_all x1, waiting for transfers between devices, on_device(): piece = lax.all_to_all(piece, 'fs', 0, 0, tiled=True)  51.7 us
    all_to_all x1, starting transfers between devices, on_device(): piece = lax.all_to_all(piece, 'fs', 0, 0, tiled=True)  47.3 us
    reduce_scatter x1, waiting for transfers between devices, on_device(): lax.psum_scatter(partial, 'fs', scatter_dimension=0, tiled=True, axis_ind...  40.5 us
    all_to_all x1, waiting for transfers between devices, on_device(): common = lax.all_to_all(common, 'tp', 0, 0, tiled=True)  10.8 us
    concatenate x1, local copies, waits for them, and re-layouts, on_device(): inward = jnp.concatenate([own[:, :2 * hid], other[:, :2 * hid]], axis=1)  8.1 us
    dot_general x3, matrix products, mm(): return jnp.dot(a, b, preferred_element_type=F32)  7.99 us
  transfers between devices with their start and end apart: 9, of which 8 were waited for; matrix products, arithmetic and copies ran while one was open for 11% of the time, Pallas kernels for 0%

profile of v4, /device:TPU:40, one launch (start us, length us, event | category | flops | bytes accessed | tf_op | source)
XLA Modules:
  0.0 383.1 jit_solution(9779132913093456738)
XLA Ops:
  7.2 4.7 %all-to-all-start = ((bf16[4,32,512]{2,1,0:T(8,128)(2,1)}), bf16[4,32,512]{2,1,0:T(8,128)(2,1)S(1)}, u32[]{:S(2)}, u32[]{:S(2)}) async-start(bf16[4,32,512]{2,1,0:T(8,128)(2,1)} %bitcast.99), calls=%async_computation | async-start | bytes 262144 | tf_op jit(solution)/shard_map/all_to_all | solution.py:71
  11.9 0.8 dynamic-slice_reduce_fusion
  12.7 0.8 divide_multiply_fusion
  13.5 0.1 copy.24
  13.6 0.1 constant_dynamic-slice_fusion
  13.6 0.1 copy.23
  13.7 0.1 select_reduce_fusion
  13.9 1.3 convert_element_type.74
  15.3 1.0 multiply_convert_fusion
  16.2 1.4 fusion.20
  17.6 0.3 all-to-all-done
  17.9 0.1 convert_reduce_fusion.1
  18.1 0.8 fusion.23
  18.8 0.8 slice_bitcast_fusion.2
  19.7 0.7 concatenate.63
  20.4 47.3 %all-to-all-start.1 = ((bf16[64,24,128]{2,1,0:T(8,128)(2,1)}), bf16[64,24,128]{2,1,0:T(8,128)(2,1)S(1)}, u32[]{:S(2)}, u32[]{:S(2)}) async-start(bf16[64,24,128]{2,1,0:T(8,128)(2,1)} %fusion.20), calls=%async_computation.1 | async-start | bytes 786432 | tf_op jit(solution)/shard_map/weights/all_to_all | solution.py:100
  67.7 0.1 all-gather.3.cloned.1.call-start
  67.8 0.7 all-gather.3.cloned.1.call-update
  68.6 51.7 %all-to-all-done.1 = bf16[64,24,128]{2,1,0:T(8,128)(2,1)S(1)} async-done(((bf16[64,24,128]{2,1,0:T(8,128)(2,1)}), bf16[64,24,128]{2,1,0:T(8,128)(2,1)S(1)}, u32[]{:S(2)}, u32[]{:S(2)}) %all-to-all-start.1) | async-done | bytes 393248 | tf_op jit(solution)/shard_map/weights/all_to_all | solution.py:100
  120.3 0.1 broadcast_in_dim.62
  120.4 11.4 %all_to_all.40 = bf16[2,64,24,128]{3,2,1,0:T(8,128)(2,1)S(1)} all-to-all(bf16[2,64,24,128]{3,2,1,0:T(8,128)(2,1)S(1)} %broadcast_in_dim.62), channel_id=1, replica_groups=mesh['grp'=2,'fs'=64,'tp'=4] {'grp'}, dimensions={0} | all-to-all | bytes 1572864 | tf_op jit(solution)/shard_map/weights/all_to_all | solution.py:14
  131.8 0.1 slice_bitcast_fusion.1
  131.9 0.1 pad_maximum_fusion
  132.0 0.4 broadcast_in_dim.63
  132.4 40.8 %all_to_all.41 = bf16[4,64,48,128]{3,2,1,0:T(8,128)(2,1)S(1)} all-to-all(bf16[4,64,48,128]{3,2,1,0:T(8,128)(2,1)S(1)} %broadcast_in_dim.63), channel_id=1, replica_groups=mesh['grp'=2,'fs'=64,'tp'=4] {'tp'}, dimensions={0} | all-to-all | bytes 6291456 | tf_op jit(solution)/shard_map/weights/all_to_all | solution.py:14
  173.2 0.5 fusion.34
  173.7 1.6 pad_maximum_fusion.1
  175.3 2.6 fusion.35
  177.9 7.0 %concatenate.69 = bf16[2048,768]{1,0:T(8,128)(2,1)S(1)} concatenate(bf16[2048,64]{1,0:T(8,128)(2,1)} %bitcast.75, bf16[2048,64]{1,0:T(8,128)(2,1)} %bitcast.73, bf16[2048,64]{1,0:T(8,128)(2,1)} %bitcast.71, bf16[2048,64]{1,0:T(8,128)(2,1)} %bitcast.69, bf16[2048,64]{1,0:T(8,128)(2,1)} %bitcast.67, bf16[2048,64]{1,0:T(8,128)(2,1)} %bitcast.65, bf16[2048,64]{1,0:T(8,128)(2,1)} %bitcast.63, ...), dimensions={1} | concatenate | bytes 6291456 | tf_op jit(solution)/shard_map/concatenate | solution.py:104
  184.9 2.1 collective-permute-start
  187.1 0.1 multiply_convert_fusion.3
  187.2 0.1 maximum_maximum_fusion
  187.3 5.3 %collective-permute-done = bf16[2048,768]{1,0:T(8,128)(2,1)} collective-permute-done((bf16[2048,768]{1,0:T(8,128)(2,1)S(1)}, bf16[2048,768]{1,0:T(8,128)(2,1)}, u32[]{:S(2)}, u32[]{:S(2)}) %collective-permute-start) | collective-permute-done | bytes 3145760 | tf_op jit(solution)/shard_map/ppermute | solution.py:105
  192.6 2.4 slice.263
  195.0 5.5 %concatenate.71 = bf16[2048,512]{1,0:T(8,128)(2,1)} concatenate(bf16[2048,64]{1,0:T(8,128)(2,1)} %bitcast.80, bf16[2048,64]{1,0:T(8,128)(2,1)} %bitcast.82, bf16[2048,64]{1,0:T(8,128)(2,1)} %bitcast.84, bf16[2048,64]{1,0:T(8,128)(2,1)} %bitcast.78, bf16[2048,256]{1,0:T(8,128)(2,1)} %slice.263), dimensions={1} | concatenate | bytes 4194304 | tf_op jit(solution)/shard_map/concatenate | solution.py:108
  200.4 1.8 slice.262
  202.3 8.1 %concatenate.70 = bf16[2048,1024]{1,0:T(8,128)(2,1)} concatenate(bf16[2048,64]{1,0:T(8,128)(2,1)} %bitcast.76, bf16[2048,64]{1,0:T(8,128)(2,1)} %bitcast.74, bf16[2048,64]{1,0:T(8,128)(2,1)} %bitcast.72, bf16[2048,64]{1,0:T(8,128)(2,1)} %bitcast.70, bf16[2048,64]{1,0:T(8,128)(2,1)} %bitcast.68, bf16[2048,64]{1,0:T(8,128)(2,1)} %bitcast.66, bf16[2048,64]{1,0:T(8,128)(2,1)S(1)} %bitcast.64, ...), dimensions={1} | concatenate | bytes 8388608 | tf_op jit(solution)/shard_map/concatenate | solution.py:107
  210.4 4.3 %all-gather.3.cloned.1.call-done = bf16[1024,2176]{1,0:T(8,128)(2,1)} async-done(((bf16[32,2176]{1,0:T(8,128)(2,1)}), bf16[1024,2176]{1,0:T(8,128)(2,1)}) %all-gather.3.cloned.1.call-update) | async-done | bytes 4456464 | tf_op jit(solution)/shard_map/tok_ag/all_gather | solution.py:98
  214.7 7.6 %fusion.2 = f32[1024,1024]{0,1:T(8,128)S(1)} fusion(bf16[2048,1024]{1,0:T(8,128)(2,1)} %concatenate.70, bf16[1024,2176]{1,0:T(8,128)(2,1)} %all-gather.3.cloned.1.call-done), kind=kOutput, calls=%fused_computation.9 | convolution fusion | flops 4296015872 | bytes 12582912 | tf_op jit(solution)/shard_map/dot_general | solution.py:20
  222.3 1.3 fusion.14
  223.7 0.7 fusion.10
  224.3 4.3 %convolution_convert_fusion = bf16[1024,2048]{1,0:T(8,128)(2,1)} fusion(bf16[2048,512]{1,0:T(8,128)(2,1)S(1)} %copy-done.4, bf16[1024,256]{0,1:T(8,128)(2,1)S(1)} %get-tuple-element.30, bf16[1024,256]{0,1:T(8,128)(2,1)S(1)} %get-tuple-element.29), kind=kOutput, calls=%fused_computation.2 | convolution fusion | flops 2151677952 | bytes 7340032 | tf_op jit(solution)/shard_map/dot_general | solution.py:24
  228.8 62.7 %all-gather = bf16[3072,128]{1,0:T(8,128)(2,1)} all-gather(bf16[48,128]{1,0:T(8,128)(2,1)S(1)} %maximum_maximum_fusion), channel_id=2, replica_groups=mesh['grp'=2,'fs'=64,'tp'=4] {'fs'}, dimensions={0}, use_global_device_ids=true | all-gather | bytes 798720 | tf_op jit(solution)/shard_map/shared/all_gather | solution.py:133
  291.4 4.3 %all-to-all-start.4 = ((bf16[4,16,48,128]{3,2,1,0:T(8,128)(2,1)}), bf16[4,16,48,128]{3,2,1,0:T(8,128)(2,1)S(1)}, u32[]{:S(2)}, u32[]{:S(2)}) async-start(bf16[4,16,48,128]{3,2,1,0:T(8,128)(2,1)} %bitcast.22), calls=%async_computation.4 | async-start | bytes 1572864 | tf_op jit(solution)/shard_map/shared/all_to_all | solution.py:135
  295.7 2.0 dynamic-slice_bitcast_fusion
  297.7 10.8 %all-to-all-done.4 = bf16[4,16,48,128]{3,2,1,0:T(8,128)(2,1)S(1)} async-done(((bf16[4,16,48,128]{3,2,1,0:T(8,128)(2,1)}), bf16[4,16,48,128]{3,2,1,0:T(8,128)(2,1)S(1)}, u32[]{:S(2)}, u32[]{:S(2)}) %all-to-all-start.4) | async-done | bytes 786464 | tf_op jit(solution)/shard_map/shared/all_to_all | solution.py:135
  308.5 3.4 all-to-all-start.5
  311.9 0.2 fusion.37
  312.1 0.2 pad_maximum_fusion.2
  312.3 0.2 pad_maximum_fusion.3
  312.5 5.2 %all-to-all-done.5 = bf16[4,32,512]{2,1,0:T(8,128)(2,1)S(1)} async-done(((bf16[4,32,512]{2,1,0:T(8,128)(2,1)}), bf16[4,32,512]{2,1,0:T(8,128)(2,1)S(1)}, u32[]{:S(2)}, u32[]{:S(2)}) %all-to-all-start.5) | async-done | bytes 131104 | tf_op jit(solution)/shard_map/shared/all_to_all | solution.py:137
  317.8 0.2 fusion.40
  318.0 0.2 fusion.41
  318.2 0.9 broadcast_in_dim.70
  319.1 3.6 all-to-all-start.6
  322.6 0.1 fusion.36
  322.8 0.1 fusion.27
  322.9 0.2 pad_maximum_fusion.4
  323.1 40.5 %reduce-scatter.2.cloned.1.call-done = bf16[32,2048]{1,0:T(8,128)(2,1)} async-done(((bf16[1024,2048]{1,0:T(8,128)(2,1)}), bf16[32,2048]{1,0:T(8,128)(2,1)}) %reduce-scatter.2.cloned.1.call-update) | async-done | bytes 131088 | tf_op jit(solution)/shard_map/rs/reduce_scatter | solution.py:129
  363.6 1.6 copy.28
  365.2 4.2 %all-to-all-start.7 = ((bf16[4,32,512]{2,1,0:T(8,128)(2,1)}), bf16[4,32,512]{2,1,0:T(8,128)(2,1)S(1)}, u32[]{:S(2)}, u32[]{:S(2)}) async-start(bf16[4,32,512]{2,1,0:T(8,128)(2,1)} %bitcast.60), calls=%async_computation.8 | async-start | bytes 262144 | tf_op jit(solution)/shard_map/all_to_all | solution.py:148
  369.4 0.1 convert_reduce_fusion
  369.5 5.9 %all-to-all-done.7 = bf16[4,32,512]{2,1,0:T(8,128)(2,1)S(1)} async-done(((bf16[4,32,512]{2,1,0:T(8,128)(2,1)}), bf16[4,32,512]{2,1,0:T(8,128)(2,1)S(1)}, u32[]{:S(2)}, u32[]{:S(2)}) %all-to-all-start.7) | async-done | bytes 131104 | tf_op jit(solution)/shard_map/all_to_all | solution.py:148
  375.4 0.9 fusion.6
  (40 shorter events, 0.3 us)
Async XLA Ops:
  7.2 6.4 %copy-start = (s32[128,8]{0,1:T(8,128)S(1)}, s32[128,8]{0,1:T(8,128)}, u32[]{:S(2)}) copy-start(s32[128,8]{0,1:T(8,128)} %param.11) | copy-start | bytes 12292
  7.2 8.0 %copy-start.8 = (f32[64,32,64]{2,1,0:T(8,128)S(1)}, f32[64,32,64]{2,1,0:T(8,128)}, u32[]{:S(2)}) copy-start(f32[64,32,64]{2,1,0:T(8,128)} %param.14) | copy-start | bytes 1572868
  7.2 8.0 %copy-start.7 = (f32[64,32,64]{2,1,0:T(8,128)S(1)}, f32[64,32,64]{2,1,0:T(8,128)}, u32[]{:S(2)}) copy-start(f32[64,32,64]{2,1,0:T(8,128)} %param.15) | copy-start | bytes 1572868
  7.2 10.7 %all-to-all-start = ((bf16[4,32,512]{2,1,0:T(8,128)(2,1)}), bf16[4,32,512]{2,1,0:T(8,128)(2,1)S(1)}, u32[]{:S(2)}, u32[]{:S(2)}) async-start(bf16[4,32,512]{2,1,0:T(8,128)(2,1)} %bitcast.99), calls=%async_computation | async-start | bytes 262144 | tf_op jit(solution)/shard_map/all_to_all | solution.py:71
  20.4 99.9 %all-to-all-start.1 = ((bf16[64,24,128]{2,1,0:T(8,128)(2,1)}), bf16[64,24,128]{2,1,0:T(8,128)(2,1)S(1)}, u32[]{:S(2)}, u32[]{:S(2)}) async-start(bf16[64,24,128]{2,1,0:T(8,128)(2,1)} %fusion.20), calls=%async_computation.1 | async-start | bytes 786432 | tf_op jit(solution)/shard_map/weights/all_to_all | solution.py:100
  67.7 146.9 %all-gather.3.cloned.1.call-start = ((), (), s32[]{:S(2)}) async-start(), calls=%async_computation.9 | async-start | bytes 4595712 | tf_op jit(solution)/shard_map/tok_ag/all_gather | solution.py:98
  68.5 295.1 %reduce-scatter.2.cloned.1.call-start = ((), (), s32[]{:S(2)}) async-start(), calls=%async_computation.10 | async-start | bytes 4325376 | tf_op jit(solution)/shard_map/rs/reduce_scatter | solution.py:129
  177.9 9.2 %copy-start.12 = (f32[32,64]{1,0:T(8,128)S(1)}, f32[32,64]{1,0:T(8,128)}, u32[]{:S(2)}) copy-start(f32[32,64]{1,0:T(8,128)} %param.19) | copy-start | bytes 24580
  177.9 9.2 %copy-start.10 = (f32[32,64]{1,0:T(8,128)S(1)}, f32[32,64]{1,0:T(8,128)}, u32[]{:S(2)}) copy-start(f32[32,64]{1,0:T(8,128)} %param.17) | copy-start | bytes 24580
  177.9 9.2 %copy-start.11 = (f32[32,64]{1,0:T(8,128)S(1)}, f32[32,64]{1,0:T(8,128)}, u32[]{:S(2)}) copy-start(f32[32,64]{1,0:T(8,128)} %param.18) | copy-start | bytes 24580
  177.9 9.2 %copy-start.13 = (f32[32]{0:T(128)S(1)}, f32[32]{0:T(128)}, u32[]{:S(2)}) copy-start(f32[32]{0:T(128)} %param.13) | copy-start | bytes 388
  184.9 10.1 %copy-start.1 = (bf16[2048,768]{1,0:T(8,128)(2,1)}, bf16[2048,768]{1,0:T(8,128)(2,1)S(1)}, u32[]{:S(2)}) copy-start(bf16[2048,768]{1,0:T(8,128)(2,1)S(1)} %concatenate.69) | copy-start | bytes 9437188
  184.9 7.7 %collective-permute-start = (bf16[2048,768]{1,0:T(8,128)(2,1)S(1)}, bf16[2048,768]{1,0:T(8,128)(2,1)}, u32[]{:S(2)}, u32[]{:S(2)}) collective-permute-start(bf16[2048,768]{1,0:T(8,128)(2,1)S(1)} %concatenate.69), channel_id=1, source_target_pairs={{0,4},{4,0},{8,12},{12,8},{16,20},{20,16},{24,28},{28,24},{32,36},... | collective-permute-start | bytes 9437192 | tf_op jit(solution)/shard_map/ppermute | solution.py:105
  200.4 1.8 copy-start.2
  200.4 1.9 copy-start.3
  222.3 2.0 copy-start.4
  291.4 17.1 %all-to-all-start.4 = ((bf16[4,16,48,128]{3,2,1,0:T(8,128)(2,1)}), bf16[4,16,48,128]{3,2,1,0:T(8,128)(2,1)S(1)}, u32[]{:S(2)}, u32[]{:S(2)}) async-start(bf16[4,16,48,128]{3,2,1,0:T(8,128)(2,1)} %bitcast.22), calls=%async_computation.4 | async-start | bytes 1572864 | tf_op jit(solution)/shard_map/shared/all_to_all | solution.py:135
  308.5 9.3 %all-to-all-start.5 = ((bf16[4,32,512]{2,1,0:T(8,128)(2,1)}), bf16[4,32,512]{2,1,0:T(8,128)(2,1)S(1)}, u32[]{:S(2)}, u32[]{:S(2)}) async-start(bf16[4,32,512]{2,1,0:T(8,128)(2,1)} %fusion.23), calls=%async_computation.5 | async-start | bytes 262144 | tf_op jit(solution)/shard_map/shared/all_to_all | solution.py:137
  312.3 10.8 %copy-start.5 = (bf16[512,256]{1,0:T(8,128)(2,1)}, bf16[512,256]{1,0:T(8,128)(2,1)S(1)}, u32[]{:S(2)}) copy-start(bf16[512,256]{1,0:T(8,128)(2,1)S(1)} %pad_maximum_fusion.2) | copy-start | bytes 786436
  312.5 52.7 %copy-start.6 = (bf16[512,256]{1,0:T(8,128)(2,1)}, bf16[512,256]{1,0:T(8,128)(2,1)S(1)}, u32[]{:S(2)}) copy-start(bf16[512,256]{1,0:T(8,128)(2,1)S(1)} %pad_maximum_fusion.3) | copy-start | bytes 786436
  319.1 46.2 %all-to-all-start.6 = ((bf16[4,128,512]{2,1,0:T(8,128)(2,1)}), bf16[4,128,512]{2,1,0:T(8,128)(2,1)S(1)}, u32[]{:S(2)}, u32[]{:S(2)}) async-start(bf16[4,128,512]{2,1,0:T(8,128)(2,1)} %broadcast_in_dim.70), calls=%async_computation.6 | async-start | bytes 1048576 | tf_op jit(solution)/shard_map/shared/all_to_all | solution.py:14
  323.1 53.2 %copy-start.9 = (bf16[512,256]{1,0:T(8,128)(2,1)}, bf16[512,256]{1,0:T(8,128)(2,1)S(1)}, u32[]{:S(2)}) copy-start(bf16[512,256]{1,0:T(8,128)(2,1)S(1)} %pad_maximum_fusion.4) | copy-start | bytes 786436
  365.2 10.2 %all-to-all-start.7 = ((bf16[4,32,512]{2,1,0:T(8,128)(2,1)}), bf16[4,32,512]{2,1,0:T(8,128)(2,1)S(1)}, u32[]{:S(2)}, u32[]{:S(2)}) async-start(bf16[4,32,512]{2,1,0:T(8,128)(2,1)} %bitcast.60), calls=%async_computation.8 | async-start | bytes 262144 | tf_op jit(solution)/shard_map/all_to_all | solution.py:148
Sparse Core Ops, SparseCore 0:
  71.2 143.4 all-gather.2
  228.9 134.7 reduce-scatter.1
